TPU v7x, 512 devices: a whole 4x8x8 slice. The times are simulated.
512 devices in a mesh: sp: 64 (over z, y), tp: 8 (over x, core).
Axes of the slice: x: 4, y: 8, z: 8, core: 2. Of those that a mesh axis runs over, the one named last changes fastest.
Arguments:
- block_input: bfloat16 [4, 4096, 4096], P(None, 'sp', 'tp'), may hold values from -6 to 6
- key_weight: bfloat16 [4096, 2048], P('sp', 'tp'), may hold values from -0.09375 to 0.09375
- value_weight: bfloat16 [4096, 2048], P('sp', 'tp'), may hold values from -0.09375 to 0.09375
- earlier_keys: bfloat16 [4, 16384, 2048], P(None, 'sp', 'tp'), may hold values from -10 to 10
- past_values: bfloat16 [4, 16384, 2048], P(None, 'sp', 'tp'), may hold values from -6 to 6
- past_gates: float32 [4, 16, 16384], P(None, 'tp', 'sp'), may hold values from -3074.15 to 0, as said below
- block_gates: float32 [4, 16, 4096], P(None, 'tp', 'sp'), may hold values from -3074.15 to 0
- step_query: bfloat16 [4, 2048], P(None, 'tp'), may hold values from -12 to 12
- step_key: bfloat16 [4, 2048], P(None, 'tp'), may hold values from -10 to 10
- step_value: bfloat16 [4, 2048], P(None, 'tp'), may hold values from -6 to 6
- step_gate: float32 [4, 16], P(None, 'tp'), may hold values from -3074.15 to 0, as said below
Outputs:
- cache_keys: bfloat16 [64, 1280, 2048], P('sp', None, 'tp')
- stored_vector_entries: bfloat16 [64, 1280, 2048], P('sp', None, 'tp')
- cache_gates: float32 [64, 16, 1280], P('sp', 'tp')
- initial_attention_output: float32 [4, 2048], P(None, 'tp')
Inputs may be any that keep to these rules, and one draw needn't show every extreme that they name: Cumulative sums of negative log gates along each sequence and head; they never rise from one position to the next, and block_gates continue past_gates. `step_gate`: the cumulative log gate one position after the block, no larger than the block's last.
All inputs are finite; a program needn't handle non-finite values.
Results may differ from a plain program's by a relative error of at most 0.0055.
Values may be sent and summed in bfloat16 or wider, within the bound.
A program may use at most 64 MiB of HBM per device.

v0:
```python
import jax
import jax.numpy as jnp
from jax import lax
from jax.sharding import PartitionSpec as P

HEAD_DIM = 128
GROUP = 16


def in_order(pieces, dim):
    shape = list(pieces.shape[1:])
    shape[dim] *= pieces.shape[0]
    return jnp.moveaxis(pieces, 0, dim).reshape(shape)


def from_everyone(array, axis):
    copies = jnp.broadcast_to(array, (lax.axis_size(axis), *array.shape))
    return lax.all_to_all(copies, axis, split_axis=0, concat_axis=0, tiled=True)


def collect(array, axis, dim):
    return in_order(from_everyone(array, axis), dim)


def sent_together(arrays, axis, dim, along):
    widths = [a.shape[along] for a in arrays]
    both = jnp.concatenate(arrays, axis=along)
    out = lax.all_gather(both, axis, axis=dim, tiled=True)
    return tuple(jnp.split(out, [sum(widths[:k]) for k in range(1, len(widths))], axis=along))


def side_by_side(arrays, axis, split_dim, concat_dim, along):
    both = jnp.concatenate(arrays, axis=along)
    out, at, gathered = (
        lax.all_to_all(both, axis, split_axis=split_dim, concat_axis=concat_dim, tiled=True),
        0,
        [],
    )
    for a in arrays:
        gathered.append(lax.slice_in_dim(out, at, at + a.shape[along], axis=along))
        at += a.shape[along]
    return tuple(gathered)


def collected_together(array, axis):
    leaves = jax.tree.leaves(array)
    turns = sorted(range(len(leaves)), key=lambda k: -leaves[k].size)
    width = (1, *leaves[turns[0]].shape)[-1]
    lines = [
        jnp.pad(leaves[k].reshape(-1), (0, -leaves[k].size % width)).reshape(-1, width)
        for k in turns
    ]
    both, at, found = (from_everyone(jnp.concatenate(lines), axis), 0, {})
    for k, line in zip(turns, lines):
        piece = both[:, at : at + len(line)].reshape(len(both), -1)
        found[k] = piece[:, : leaves[k].size].reshape(-1, *leaves[k].shape)
        at += len(line)
    numbers = iter(range(len(leaves)))
    return jax.tree.map(lambda _: found[next(numbers)], array)


def combined_pairwise(pieces, combine):
    while len(jax.tree.leaves(pieces)[0]) > 1:
        pieces = jax.vmap(combine)(
            *(jax.tree.map(lambda part: part[side::2], pieces) for side in (0, 1))
        )
    return jax.tree.map(lambda part: part[0], pieces)


def joined_all(array, axis, combine):
    pieces = collected_together(array, axis)
    return combined_pairwise(pieces, combine)


def share_split(source_rows, shares):
    return source_rows.reshape(shares, -1, source_rows.shape[2])


def partial_read(queries, key_rows, value_rows, gate_rows, gate_here):
    sequences, row_count = (key_rows.shape[0], key_rows.shape[1])
    local_heads, head_width = (queries.shape[1], queries.shape[2])
    key_rows = key_rows.reshape(sequences, row_count, local_heads, head_width)
    value_rows = value_rows.reshape(sequences, row_count, local_heads, head_width)
    scores = jnp.einsum("shd,srhd->shr", queries, key_rows, preferred_element_type=jnp.float32)
    scores = scores * head_width ** (-0.5) + gate_here[:, :, None] - gate_rows
    maximum = jnp.max(scores, axis=2)
    weights = jnp.exp(scores - maximum[:, :, None])
    denominator = jnp.sum(weights, axis=2)
    summed = jnp.einsum(
        "shr,srhd->shd", weights, value_rows.astype(jnp.float32), precision=lax.Precision.HIGHEST
    )
    return (maximum, denominator, summed)


def combine_reads(former, latter):
    maximum = jnp.maximum(former[0], latter[0])
    former_scale = jnp.exp(former[0] - maximum)
    latter_scale = jnp.exp(latter[0] - maximum)
    return (
        maximum,
        former[1] * former_scale + latter[1] * latter_scale,
        former[2] * former_scale[:, :, None] + latter[2] * latter_scale[:, :, None],
    )


def local(
    block_input,
    key_weight,
    value_weight,
    earlier_keys,
    past_values,
    past_gates,
    block_gates,
    step_query,
    step_key,
    step_value,
    step_gate,
):
    sequences, span_rows = (block_input.shape[0], block_input.shape[1])
    local_width = key_weight.shape[1]
    local_heads = local_width // HEAD_DIM
    shares = sequences * GROUP
    past_parts = past_gates.reshape(sequences, local_heads, GROUP, -1)
    block_parts = block_gates.reshape(sequences, local_heads, GROUP, -1)
    gate_block_groups = (
        jnp.concatenate([past_parts, block_parts], axis=3)
        .transpose(0, 2, 1, 3)
        .reshape(shares, local_heads, -1)
    )
    cache_gates = lax.all_to_all(gate_block_groups, "sp", split_axis=0, concat_axis=2, tiled=True)
    gathered = collect(block_input, "tp", 2)
    flat_input = gathered.reshape(sequences * span_rows, gathered.shape[2])
    pieces = sent_together((key_weight, value_weight), "sp", 0, 1)
    key_sums = jnp.dot(flat_input, pieces[0], preferred_element_type=jnp.float32)
    value_sums = jnp.dot(flat_input, pieces[1], preferred_element_type=jnp.float32)
    block_keys = key_sums.astype(jnp.bfloat16).reshape(sequences, span_rows, local_width)
    block_values = value_sums.astype(jnp.bfloat16).reshape(sequences, span_rows, local_width)
    joined_keys = jnp.concatenate(
        [share_split(earlier_keys, shares), share_split(block_keys, shares)], axis=1
    )
    assembled_vector_entries = jnp.concatenate(
        [share_split(past_values, shares), share_split(block_values, shares)], axis=1
    )
    cache_keys, stored_vector_entries = side_by_side(
        (joined_keys, assembled_vector_entries), "sp", 0, 1, 2
    )
    queries = step_query.reshape(sequences, local_heads, HEAD_DIM)
    earlier = partial_read(queries, earlier_keys, past_values, past_gates, step_gate)
    recent = partial_read(queries, block_keys, block_values, block_gates, step_gate)
    merged = joined_all(combine_reads(earlier, recent), "sp", combine_reads)
    own_keys = step_key.reshape(sequences, local_heads, HEAD_DIM).astype(jnp.float32)
    own_values = step_value.reshape(sequences, local_heads, HEAD_DIM).astype(jnp.float32)
    own_score = jnp.sum(queries.astype(jnp.float32) * own_keys, axis=2) * HEAD_DIM ** (-0.5)
    maximum = jnp.maximum(merged[0], own_score)
    kept_scale = jnp.exp(merged[0] - maximum)
    fresh_weight = jnp.exp(own_score - maximum)
    denominator = merged[1] * kept_scale + fresh_weight
    summed = merged[2] * kept_scale[:, :, None] + fresh_weight[:, :, None] * own_values
    initial_attention_output = (summed / denominator[:, :, None]).reshape(sequences, local_width)
    return (cache_keys, stored_vector_entries, cache_gates, initial_attention_output)


def solution(mesh):
    in_specs = (
        P(None, "sp", "tp"),
        P("sp", "tp"),
        P("sp", "tp"),
        P(None, "sp", "tp"),
        P(None, "sp", "tp"),
        P(None, "tp", "sp"),
        P(None, "tp", "sp"),
        P(None, "tp"),
        P(None, "tp"),
        P(None, "tp"),
        P(None, "tp"),
    )
    out_specs = (P("sp", None, "tp"), P("sp", None, "tp"), P("sp", "tp", None), P(None, "tp"))
    return jax.shard_map(local, mesh=mesh, in_specs=in_specs, out_specs=out_specs, check_vma=False)
```

profile of v0, /device:TPU:6, one launch (start us, length us, event | category | flops | bytes accessed | tf_op | source)
XLA Modules:
  0.0 182.6 jit_solution(9512086993606536166)
XLA Ops:
  7.2 1.4 pad_maximum_fusion
  8.6 2.5 %broadcast_in_dim.4 = bf16[8,4,64,512]{3,2,1,0:T(8,128)(2,1)} broadcast(bf16[4,64,512]{2,1,0:T(8,128)(2,1)} %param.11), dimensions={1,2,3} | broadcast | bytes 2359296 | tf_op jit(solution)/shard_map/broadcast_in_dim | solution.py:17
  11.2 9.5 %all-to-all-start = ((bf16[8,4,64,512]{3,2,1,0:T(8,128)(2,1)}), bf16[8,4,64,512]{3,2,1,0:T(8,128)(2,1)S(1)}, u32[]{:S(2)}, u32[]{:S(2)}) async-start(bf16[8,4,64,512]{3,2,1,0:T(8,128)(2,1)} %broadcast_in_dim.4), calls=%async_computation | async-start | bytes 4194304 | tf_op jit(solution)/shard_map/all_to_all | solution.py:18
  20.7 0.1 reshape.143
  21.0 0.1 copy.98
  21.1 1.2 copy.122
  22.4 0.2 fusion.49
  22.5 0.2 fusion.43
  22.8 0.2 fusion.28
  23.0 0.8 pad_maximum_fusion.1
  23.8 0.3 fusion.16
  24.1 21.7 %all-to-all-done = bf16[8,4,64,512]{3,2,1,0:T(8,128)(2,1)S(1)} async-done(((bf16[8,4,64,512]{3,2,1,0:T(8,128)(2,1)}), bf16[8,4,64,512]{3,2,1,0:T(8,128)(2,1)S(1)}, u32[]{:S(2)}, u32[]{:S(2)}) %all-to-all-start) | async-done | bytes 2097184 | tf_op jit(solution)/shard_map/all_to_all | solution.py:18
  45.8 12.0 %all-to-all-start.2 = ((f32[64,2,20]{2,1,0:T(2,128)}), f32[64,2,20]{2,1,0:T(2,128)S(1)}, u32[]{:S(2)}, u32[]{:S(2)}) async-start(f32[64,2,20]{2,1,0:T(2,128)} %bitcast.6), calls=%async_computation.2 | async-start | bytes 131072 | tf_op jit(solution)/shard_map/all_to_all | solution.py:130
  57.8 1.2 copy.94
  59.0 0.9 copy.132
  59.9 43.1 %all-gather.2.cloned.1.call-done = bf16[4096,512]{1,0:T(8,128)(2,1)} async-done(((bf16[64,512]{1,0:T(8,128)(2,1)}), bf16[4096,512]{1,0:T(8,128)(2,1)}) %all-gather.2.cloned.1.call-update) | async-done | bytes 4194320 | tf_op jit(solution)/shard_map/all_gather | solution.py:28
  103.0 2.3 %fusion.13 = bf16[256,256]{1,0:T(8,128)(2,1)S(1)} fusion(bf16[256,4096]{1,0:T(8,128)(2,1)S(1)} %bitcast.99, bf16[4096,512]{1,0:T(8,128)(2,1)} %all-gather.2.cloned.1.call-done), kind=kOutput, calls=%fused_computation.8 | convolution fusion | flops 536936448 | bytes 4325376 | tf_op jit(solution)/shard_map/dot_general | solution.py:134
  105.4 0.2 fusion.22
  105.5 0.2 fusion.40
  105.7 0.2 fusion.45
  106.1 2.3 %fusion.10 = bf16[256,256]{1,0:T(8,128)(2,1)S(1)} fusion(bf16[256,4096]{1,0:T(8,128)(2,1)S(1)} %bitcast.100, bf16[4096,512]{1,0:T(8,128)(2,1)} %all-gather.2.cloned.1.call-done), kind=kOutput, calls=%fused_computation.7 | convolution fusion | flops 536936448 | bytes 4325376 | tf_op jit(solution)/shard_map/dot_general | solution.py:135
  108.5 0.2 fusion.20
  108.8 0.8 broadcast_in_dim.5
  109.6 8.3 %all-to-all-start.3 = ((f32[64,10,128]{2,1,0:T(8,128)}), f32[64,10,128]{2,1,0:T(8,128)S(1)}, u32[]{:S(2)}, u32[]{:S(2)}) async-start(f32[64,10,128]{2,1,0:T(8,128)} %broadcast_in_dim.5), calls=%async_computation.3 | async-start | bytes 1048576 | tf_op jit(solution)/shard_map/all_to_all | solution.py:18
  118.0 0.1 multiply_reduce_fusion
  118.1 0.7 all_to_all.34
  118.9 1.3 maximum_maximum_fusion
  120.2 13.5 %all-to-all-done.3 = f32[64,10,128]{2,1,0:T(8,128)S(1)} async-done(((f32[64,10,128]{2,1,0:T(8,128)}), f32[64,10,128]{2,1,0:T(8,128)S(1)}, u32[]{:S(2)}, u32[]{:S(2)}) %all-to-all-start.3) | async-done | bytes 327712 | tf_op jit(solution)/shard_map/all_to_all | solution.py:18
  133.7 5.0 %all-to-all-start.1 = ((bf16[64,20,512]{2,1,0:T(8,128)(2,1)}), bf16[64,20,512]{2,1,0:T(8,128)(2,1)S(1)}, u32[]{:S(2)}, u32[]{:S(2)}) async-start(bf16[64,20,512]{2,1,0:T(8,128)(2,1)} %maximum_maximum_fusion), calls=%async_computation.1 | async-start | bytes 3145728 | tf_op jit(solution)/shard_map/all_to_all | solution.py:35
  138.8 0.1 copy.128
  138.9 0.1 slice.167
  139.0 0.1 slice.166
  139.1 0.1 copy.124
  139.2 0.1 slice.141
  139.4 0.1 slice.142
  139.5 0.1 copy.130
  139.6 0.1 copy.129
  139.7 0.1 copy.125
  139.8 0.1 copy.126
  140.1 0.1 copy.110
  140.2 0.1 copy.106
  140.5 0.2 fusion.19
  140.8 0.1 multiply_add_fusion
  140.9 0.1 multiply_add_fusion.2
  141.2 0.7 bitcast_divide_fusion
  141.8 32.5 %all-to-all-done.1 = bf16[64,20,512]{2,1,0:T(8,128)(2,1)S(1)} async-done(((bf16[64,20,512]{2,1,0:T(8,128)(2,1)}), bf16[64,20,512]{2,1,0:T(8,128)(2,1)S(1)}, u32[]{:S(2)}, u32[]{:S(2)}) %all-to-all-start.1) | async-done | bytes 1310752 | tf_op jit(solution)/shard_map/all_to_all | solution.py:35
  174.3 0.3 all_to_all.30
  174.6 1.1 fusion.46
  (57 shorter events, 1.5 us)
Async XLA Ops:
  7.2 95.9 %all-gather.2.cloned.1.call-start = ((), (), s32[]{:S(2)}) async-start(), calls=%async_computation.4 | async-start | bytes 4259840 | tf_op jit(solution)/shard_map/all_gather | solution.py:28
  11.2 9.5 %copy-start.2 = (f32[4,2,64]{2,1,0:T(2,128)S(1)}, f32[4,2,64]{2,1,0:T(2,128)}, u32[]{:S(2)}) copy-start(f32[4,2,64]{2,1,0:T(2,128)} %param.17) | copy-start | bytes 6148
  11.2 9.7 %copy-start.3 = (f32[4,2,256]{2,1,0:T(2,128)S(1)}, f32[4,2,256]{2,1,0:T(2,128)}, u32[]{:S(2)}) copy-start(f32[4,2,256]{2,1,0:T(2,128)} %param.16) | copy-start | bytes 24580
  11.2 9.8 %copy-start.7 = (f32[4,2]{0,1:T(2,128)S(1)}, f32[4,2]{0,1:T(2,128)}, u32[]{:S(2)}) copy-start(f32[4,2]{0,1:T(2,128)} %param.21) | copy-start | bytes 100
  11.2 9.9 %copy-start.4 = (bf16[4,256]{1,0:T(4,128)(2,1)S(1)}, bf16[4,256]{1,0:T(4,128)(2,1)}, u32[]{:S(2)}) copy-start(bf16[4,256]{1,0:T(4,128)(2,1)} %param.18) | copy-start | bytes 6148
  11.2 34.6 %all-to-all-start = ((bf16[8,4,64,512]{3,2,1,0:T(8,128)(2,1)}), bf16[8,4,64,512]{3,2,1,0:T(8,128)(2,1)S(1)}, u32[]{:S(2)}, u32[]{:S(2)}) async-start(bf16[8,4,64,512]{3,2,1,0:T(8,128)(2,1)} %broadcast_in_dim.4), calls=%async_computation | async-start | bytes 4194304 | tf_op jit(solution)/shard_map/all_to_all | solution.py:18
  20.7 3.1 %copy-start = (bf16[4,256,256]{2,1,0:T(8,128)(2,1)S(1)}, bf16[4,256,256]{2,1,0:T(8,128)(2,1)}, u32[]{:S(2)}) copy-start(bf16[4,256,256]{2,1,0:T(8,128)(2,1)} %param.15) | copy-start | bytes 1572868
  45.8 63.0 %all-to-all-start.2 = ((f32[64,2,20]{2,1,0:T(2,128)}), f32[64,2,20]{2,1,0:T(2,128)S(1)}, u32[]{:S(2)}, u32[]{:S(2)}) async-start(f32[64,2,20]{2,1,0:T(2,128)} %bitcast.6), calls=%async_computation.2 | async-start | bytes 131072 | tf_op jit(solution)/shard_map/all_to_all | solution.py:130
  106.1 11.9 %copy-start.6 = (bf16[4,256]{1,0:T(4,128)(2,1)S(1)}, bf16[4,256]{1,0:T(4,128)(2,1)}, u32[]{:S(2)}) copy-start(bf16[4,256]{1,0:T(4,128)(2,1)} %param.19) | copy-start | bytes 6148
  108.4 10.5 %copy-start.1 = (bf16[4,256,256]{2,1,0:T(8,128)(2,1)S(1)}, bf16[4,256,256]{2,1,0:T(8,128)(2,1)}, u32[]{:S(2)}) copy-start(bf16[4,256,256]{2,1,0:T(8,128)(2,1)} %param.14) | copy-start | bytes 1572868
  109.6 24.1 %all-to-all-start.3 = ((f32[64,10,128]{2,1,0:T(8,128)}), f32[64,10,128]{2,1,0:T(8,128)S(1)}, u32[]{:S(2)}, u32[]{:S(2)}) async-start(f32[64,10,128]{2,1,0:T(8,128)} %broadcast_in_dim.5), calls=%async_computation.3 | async-start | bytes 1048576 | tf_op jit(solution)/shard_map/all_to_all | solution.py:18
  133.7 40.6 %all-to-all-start.1 = ((bf16[64,20,512]{2,1,0:T(8,128)(2,1)}), bf16[64,20,512]{2,1,0:T(8,128)(2,1)S(1)}, u32[]{:S(2)}, u32[]{:S(2)}) async-start(bf16[64,20,512]{2,1,0:T(8,128)(2,1)} %maximum_maximum_fusion), calls=%async_computation.1 | async-start | bytes 3145728 | tf_op jit(solution)/shard_map/all_to_all | solution.py:35
  138.7 2.5 %copy-start.5 = (bf16[4,256]{1,0:T(4,128)(2,1)S(1)}, bf16[4,256]{1,0:T(4,128)(2,1)}, u32[]{:S(2)}) copy-start(bf16[4,256]{1,0:T(4,128)(2,1)} %param.20) | copy-start | bytes 6148
Sparse Core Ops, SparseCore 0:
  11.6 91.3 all-gather.1
where the time goes:
time: 183 us
  waiting for transfers between devices  111 us (61%)
  starting transfers between devices  34.9 us (19%)
  between operations  14.4 us (8%)
  local copies, waits for them, and re-layouts  11.3 us (6%)
  other arithmetic  5.79 us (3%)
  matrix products  5.46 us (3%)
    all_gather x1, waiting for transfers between devices, sent_together(): out = lax.all_gather(both, axis, axis=dim, tiled=True)  43.1 us
    all_to_all x2, waiting for transfers between devices, from_everyone(): return lax.all_to_all(copies, axis, split_axis=0, concat_axis=0, tiled=True)  35.2 us
    all_to_all x1, waiting for transfers between devices, side_by_side(): lax.all_to_all(both, axis, split_axis=split_dim, concat_axis=concat_dim,...  32.5 us
    all_to_all x2, starting transfers between devices, from_everyone(): return lax.all_to_all(copies, axis, split_axis=0, concat_axis=0, tiled=True)  17.8 us
    all_to_all x1, starting transfers between devices, local(): lax.all_to_all(gate_block_groups, 'sp', split_axis=0, concat_axis=2, tile...  12 us
    all_to_all x1, starting transfers between devices, side_by_side(): lax.all_to_all(both, axis, split_axis=split_dim, concat_axis=concat_dim,...  4.98 us
  transfers between devices with their start and end apart: 5, of which 4 were waited for; matrix products, arithmetic and copies ran while one was open for 10% of the time, Pallas kernels for 0%

commit v1 on v0

v1 whole, which is shorter than its diff:
```python
import functools

import jax
import jax.numpy as jnp
from jax import lax
from jax.experimental import pallas as pl
from jax.experimental.pallas import tpu as pltpu
from jax.sharding import PartitionSpec as P

HEAD_DIM = 128
GROUP = 16
NZ = 8
NY = 8
NSP = 64
NX = 4
MESH = pl.DeviceIdType.MESH
VMEM = pltpu.VMEM

OFFS = (0, -1, 1, -2, 2, -3, 3, -4)


def remote(src, dst, send, recv, sp, tp):
    return pltpu.make_async_remote_copy(
        src_ref=src,
        dst_ref=dst,
        send_sem=send,
        recv_sem=recv,
        device_id=(sp, tp),
        device_id_type=MESH,
    )


def wait_bytes(ref, sem):
    pltpu.make_async_copy(ref, ref, sem).wait()


def move_kernel(
    k_ref,
    v_ref,
    x_ref,
    g_ref,
    w_ref,
    kv_ref,
    xg_ref,
    go_ref,
    wo_ref,
    src_ref,
    load_sem,
    kv_send,
    kv_recv,
    x_send,
    x_recv,
    g_send,
    g_recv,
    w_send,
    w_recv,
    s_send,
    s_recv,
):
    sp = lax.axis_index("sp")
    tp = lax.axis_index("tp")
    z, y = sp // NY, lax.rem(sp, NY)
    x, c = tp // 2, lax.rem(tp, 2)

    def at(h, pa, pb):
        pa = lax.rem(pa + 16, 8)
        pb = lax.rem(pb + 16, 8)
        return pa * 8 + pb if h == 0 else pb * 8 + pa

    def peer(d):
        dz, dy = d // NY, lax.rem(d, NY)
        return lax.rem(z + dz, NZ) * NY + lax.rem(y + dy, NY)

    tp_next = lax.rem(x + 1, NX) * 2 + c
    tp_prev = lax.rem(x + NX - 1, NX) * 2 + c
    tp_far = lax.rem(x + 2, NX) * 2 + c
    tp_mate = x * 2 + (1 - c)

    loads = [
        pltpu.make_async_copy(k_ref, src_ref.at[:, 0], load_sem.at[0]),
        pltpu.make_async_copy(v_ref, src_ref.at[:, 1], load_sem.at[1]),
    ]
    for load in loads:
        load.start()

    barrier = pltpu.get_barrier_semaphore()

    def greet(d, carry):
        pl.semaphore_signal(barrier, inc=1, device_id=(peer(d), tp), device_id_type=MESH)
        return carry

    lax.fori_loop(1, NSP, greet, 0)
    for other in (tp_next, tp_prev, tp_mate):
        pl.semaphore_signal(barrier, inc=1, device_id=(sp, other), device_id_type=MESH)
    pl.semaphore_wait(barrier, NSP - 1 + 3)

    for load in loads:
        load.wait()

    pos = ((z, y), (y, z))

    def w_copy(h, i, pa, pb):
        chunk = wo_ref.at[i, h]
        return remote(chunk, chunk, w_send.at[h], w_recv.at[h, i], at(h, pa, pb), tp)

    def w_wait(h, i):
        wait_bytes(wo_ref.at[i, h], w_recv.at[h, i])

    wo_ref[sp] = w_ref[...]

    def first_axis(h, off_src, step):
        pa, pb = pos[h]
        w_copy(h, at(h, pa + off_src, pb), pa + step, pb).start()

    def second_axis(h, off, dist, step):
        pa, pb = pos[h]
        w_copy(h, at(h, pa + off, pb - dist * step), pa, pb + step).start()

    for h in (0, 1):
        pa, pb = pos[h]
        for step in (1, -1):
            i = at(h, pa, pb)
            remote(w_ref.at[h], wo_ref.at[i, h], w_send.at[h], w_recv.at[h, i], at(h, pa + step, pb), tp).start()

    def send_block(d, carry):
        dest = peer(d)
        remote(x_ref.at[dest], xg_ref.at[tp, sp], x_send, x_recv, dest, tp).start()
        remote(g_ref.at[dest], go_ref.at[sp], g_send, g_recv, dest, tp).start()
        return carry

    lax.fori_loop(1, NSP, send_block, 0)
    xg_ref[tp, sp] = x_ref[sp]
    go_ref[sp] = g_ref[sp]
    kv_ref[sp] = src_ref[sp]

    for h in (0, 1):
        pa, pb = pos[h]
        for step in (1, -1):
            i = at(h, pa, pb)
            remote(w_ref.at[h], wo_ref.at[i, h], w_send.at[h], w_recv.at[h, i], at(h, pa, pb + step), tp).start()

    for dist in (1, 2, 3, 4):
        for h in (0, 1):
            pa, pb = pos[h]
            for step in (1, -1):
                if dist == 4 and step == -1:
                    continue
                off = -dist * step
                w_wait(h, at(h, pa + off, pb))
                if dist < (4 if step == 1 else 3):
                    first_axis(h, off, step)
                for side in (1, -1):
                    second_axis(h, off, 0, side)

    def send_past(d, carry):
        dest = peer(d)
        remote(src_ref.at[dest], kv_ref.at[sp], kv_send, kv_recv, dest, tp).start()
        return carry

    def slab_copy(t, lo, n, k, other):
        ref = xg_ref.at[t, pl.ds(lo, n)]
        return remote(ref, ref, s_send.at[k], s_recv.at[k], sp, other)

    def second_round(dist):
        for n, off in enumerate(OFFS):
            for h in (0, 1):
                pa, pb = pos[h]
                for step in (1, -1):
                    w_wait(h, at(h, pa + off, pb - dist * step))
                    if dist < 3 or (step == 1) == (off % 2 == 0):
                        second_axis(h, off, dist, step)

    second_round(1)

    wait_bytes(xg_ref.at[tp, pl.ds(0, NSP - 1)], x_recv)
    slabs = [slab_copy(tp, 0, NSP, 0, tp_next), slab_copy(tp, 0, NSP, 1, tp_prev), slab_copy(tp, 0, NSP, 2, tp_mate)]
    for s in slabs:
        s.start()
    second_round(2)
    wait_bytes(xg_ref.at[tp_prev], s_recv.at[0])
    wait_bytes(xg_ref.at[tp_next], s_recv.at[1])
    more = [
        slab_copy(tp_prev, 0, NSP // 2, 3, tp_next),
        slab_copy(tp_next, NSP // 2, NSP // 2, 4, tp_prev),
        slab_copy(tp_prev, 0, NSP, 5, tp_mate),
        slab_copy(tp_next, 0, NSP, 6, tp_mate),
    ]
    for s in more:
        s.start()
    second_round(3)
    lax.fori_loop(1, NSP, send_past, 0)
    wait_bytes(xg_ref.at[tp_far, pl.ds(0, NSP // 2)], s_recv.at[3])
    wait_bytes(xg_ref.at[tp_far, pl.ds(0, NSP // 2)], s_recv.at[4])
    last = [slab_copy(tp_far, 0, NSP, 7, tp_mate)]
    for s in last:
        s.start()
    for k in (2, 5, 6, 7):
        wait_bytes(xg_ref.at[tp_mate], s_recv.at[k])
    for n, off in enumerate(OFFS):
        for h in (0, 1):
            pa, pb = pos[h]
            w_wait(h, at(h, pa + off, pb + 4))

    for s in slabs + more + last:
        s.wait_send()
    for h in (0, 1):
        wait_bytes(wo_ref.at[pl.ds(0, NSP - 1), 0], w_send.at[h])
    wait_bytes(xg_ref.at[tp, pl.ds(0, NSP - 1)], x_send)
    wait_bytes(go_ref.at[pl.ds(0, NSP - 1)], g_send)
    wait_bytes(go_ref.at[pl.ds(0, NSP - 1)], g_recv)
    wait_bytes(kv_ref.at[pl.ds(0, NSP - 1)], kv_send)
    wait_bytes(kv_ref.at[pl.ds(0, NSP - 1)], kv_recv)


def move(k, v, xb, g, w):
    vm = pl.BlockSpec(memory_space=VMEM)
    dma = pltpu.SemaphoreType.DMA
    return pl.pallas_call(
        move_kernel,
        out_shape=(
            jax.ShapeDtypeStruct((NSP, 2, 16, 256), jnp.bfloat16),
            jax.ShapeDtypeStruct((8, NSP, 16, 128), jnp.bfloat16),
            jax.ShapeDtypeStruct((NSP, 1, 128), jnp.float32),
            jax.ShapeDtypeStruct((NSP, 2, 32, 512), jnp.bfloat16),
        ),
        in_specs=[pl.BlockSpec(memory_space=pl.ANY)] * 2 + [vm] * 3,
        out_specs=(vm,) * 4,
        scratch_shapes=[
            VMEM((NSP, 2, 16, 256), jnp.bfloat16),
            dma((2,)),
            dma,
            dma,
            dma,
            dma,
            dma,
            dma,
            dma((2,)),
            dma((2, NSP)),
            dma((8,)),
            dma((8,)),
        ],
        compiler_params=pltpu.CompilerParams(
            collective_id=0, has_side_effects=True, vmem_limit_bytes=40 * 1024 * 1024
        ),
    )(k, v, xb, g, w)


def share_kernel(o_ref, m_ref, oo_ref, mo_ref, sends, recvs):
    sp = lax.axis_index("sp")
    tp = lax.axis_index("tp")

    barrier = pltpu.get_barrier_semaphore()

    def greet(d, carry):
        pl.semaphore_signal(barrier, inc=1, device_id=(lax.rem(sp + d, NSP), tp), device_id_type=MESH)
        return carry

    lax.fori_loop(1, NSP, greet, 0)
    pl.semaphore_wait(barrier, NSP - 1)

    def send(d, carry):
        dest = lax.rem(sp + d, NSP)
        remote(o_ref, oo_ref.at[sp], sends.at[0], recvs.at[0], dest, tp).start()
        remote(m_ref, mo_ref.at[sp], sends.at[1], recvs.at[1], dest, tp).start()
        return carry

    lax.fori_loop(1, NSP, send, 0)
    oo_ref[sp] = o_ref[...]
    mo_ref[sp] = m_ref[...]
    for sem in (sends, recvs):
        wait_bytes(oo_ref.at[pl.ds(0, NSP - 1)], sem.at[0])
        wait_bytes(mo_ref.at[pl.ds(0, NSP - 1)], sem.at[1])


def share(o, m):
    vm = pl.BlockSpec(memory_space=VMEM)
    dma = pltpu.SemaphoreType.DMA
    return pl.pallas_call(
        share_kernel,
        out_shape=(
            jax.ShapeDtypeStruct((NSP, *o.shape), jnp.float32),
            jax.ShapeDtypeStruct((NSP, *m.shape), jnp.float32),
        ),
        in_specs=[vm] * 2,
        out_specs=(vm,) * 2,
        scratch_shapes=[dma((2,)), dma((2,))],
        compiler_params=pltpu.CompilerParams(collective_id=1, has_side_effects=True),
    )(o, m)


def partial_read(queries, key_rows, value_rows, gate_rows, gate_here):
    scores = jnp.einsum("shd,srhd->shr", queries, key_rows, preferred_element_type=jnp.float32)
    scores = scores * HEAD_DIM ** (-0.5) + gate_here[:, :, None] - gate_rows
    maximum = jnp.max(scores, axis=2)
    weights = jnp.exp(scores - maximum[:, :, None])
    denominator = jnp.sum(weights, axis=2)
    summed = jnp.einsum(
        "shr,srhd->shd", weights, value_rows.astype(jnp.float32), precision=lax.Precision.HIGHEST
    )
    return (maximum, denominator, summed)


def local(
    block_input,
    key_weight,
    value_weight,
    earlier_keys,
    past_values,
    past_gates,
    block_gates,
    step_query,
    step_key,
    step_value,
    step_gate,
):
    seqs = block_input.shape[0]
    heads = 2
    sp = lax.axis_index("sp")
    xb = block_input.reshape(seqs, GROUP, 4, 4, 128).transpose(0, 1, 3, 2, 4).reshape(NSP, 16, 128)
    past_parts = past_gates.reshape(seqs, heads, GROUP, 16)
    block_parts = block_gates.reshape(seqs, heads, GROUP, 4)
    gates = jnp.concatenate([past_parts, block_parts], axis=3).transpose(0, 2, 1, 3).reshape(NSP, 1, 40)
    gates = jnp.pad(gates, ((0, 0), (0, 0), (0, 88)))
    w = jnp.concatenate([key_weight, value_weight], axis=1).reshape(2, 32, 512)
    kv, xg, go, wo = move(
        earlier_keys.reshape(NSP, 16, 256), past_values.reshape(NSP, 16, 256), xb, gates, w
    )
    go = go[:, 0, :40].reshape(NSP, heads, 20)
    cache_gates = go.transpose(1, 0, 2).reshape(1, heads, NSP * 20)
    rows = xg.reshape(8, NSP, 4, 4, 128).transpose(1, 3, 0, 2, 4).reshape(256, 4096)
    kvb = jnp.dot(rows, wo.reshape(4096, 512), preferred_element_type=jnp.float32).astype(jnp.bfloat16)
    kb, vb = kvb[:, :256], kvb[:, 256:]
    cache_keys = jnp.concatenate([kv[:, 0], kb.reshape(NSP, 4, 256)], axis=1).reshape(1, 1280, 256)
    cache_values = jnp.concatenate([kv[:, 1], vb.reshape(NSP, 4, 256)], axis=1).reshape(1, 1280, 256)

    queries = step_query.reshape(seqs, heads, HEAD_DIM)
    m0, l0, o0 = partial_read(
        queries,
        earlier_keys.reshape(seqs, 256, heads, HEAD_DIM),
        past_values.reshape(seqs, 256, heads, HEAD_DIM),
        past_gates,
        step_gate,
    )
    seq = sp // GROUP
    q1 = lax.dynamic_slice_in_dim(queries, seq, 1, 0)
    s1 = lax.dynamic_slice_in_dim(step_gate, seq, 1, 0)
    g1 = go[:, :, 16:].transpose(1, 0, 2).reshape(1, heads, 256)
    m1, l1, o1 = partial_read(
        q1, kb.reshape(1, 256, heads, HEAD_DIM), vb.reshape(1, 256, heads, HEAD_DIM), g1, s1
    )
    mine = (jnp.arange(seqs) == seq)[:, None]
    mx = jnp.where(mine, jnp.maximum(m0, m1), m0)
    f0 = jnp.exp(m0 - mx)
    f1 = jnp.where(mine, jnp.exp(m1 - mx), 0.0)
    den = l0 * f0 + l1 * f1
    summed = o0 * f0[:, :, None] + o1 * f1[:, :, None]
    ml = jnp.concatenate([mx.reshape(1, 8), den.reshape(1, 8), jnp.zeros((1, 112), jnp.float32)], axis=1)
    oo, mo = share(summed.reshape(8, HEAD_DIM), ml)
    mall = mo[:, 0, :8]
    lall = mo[:, 0, 8:16]
    own_keys = step_key.reshape(seqs, heads, HEAD_DIM).astype(jnp.float32)
    own_values = step_value.reshape(8, HEAD_DIM).astype(jnp.float32)
    own_score = (jnp.sum(queries.astype(jnp.float32) * own_keys, axis=2) * HEAD_DIM ** (-0.5)).reshape(8)
    top = jnp.maximum(jnp.max(mall, axis=0), own_score)
    fs = jnp.exp(mall - top)
    own = jnp.exp(own_score - top)
    den = jnp.sum(lall * fs, axis=0) + own
    out = jnp.sum(oo * fs[:, :, None], axis=0) + own[:, None] * own_values
    attention = (out / den[:, None]).reshape(seqs, heads * HEAD_DIM)
    return (cache_keys, cache_values, cache_gates, attention)


def solution(mesh):
    in_specs = (
        P(None, "sp", "tp"),
        P("sp", "tp"),
        P("sp", "tp"),
        P(None, "sp", "tp"),
        P(None, "sp", "tp"),
        P(None, "tp", "sp"),
        P(None, "tp", "sp"),
        P(None, "tp"),
        P(None, "tp"),
        P(None, "tp"),
        P(None, "tp"),
    )
    out_specs = (P("sp", None, "tp"), P("sp", None, "tp"), P("sp", "tp", None), P(None, "tp"))
    return jax.shard_map(local, mesh=mesh, in_specs=in_specs, out_specs=out_specs, check_vma=False)
```

time: 183 us -> 134 us (0.73); the launches traced: 183 us -> 132 us
  waiting for transfers between devices: 111 us -> 0 us
  Pallas kernels: 0 us -> 100 us
  starting transfers between devices: 34.9 us -> 0 us
  between operations: 14.4 us -> 0.91 us
  local copies, waits for them, and re-layouts: 11.3 us -> 17.8 us
  other arithmetic: 5.79 us -> 7.63 us
    pallas_call x0 -> x2, Pallas kernels: none -> 100 us  [the longest x1 80.7 us: move(): pl.pallas_call(move_kernel, out_shape=(jax.ShapeDtypeStruct((NSP, 2, 16,...]
    all_to_all x4 -> x0, waiting for transfers between devices: 67.7 us -> none  [the longest x2 35.2 us: from_everyone(): return lax.all_to_all(copies, axis, split_axis=0, concat_axis=0, tiled=True)]
    all_gather x1 -> x0, waiting for transfers between devices: 43.1 us -> none  [sent_together(): out = lax.all_gather(both, axis, axis=dim, tiled=True)]
    all_to_all x4 -> x0, starting transfers between devices: 34.8 us -> none  [the longest x2 17.8 us: from_everyone(): return lax.all_to_all(copies, axis, split_axis=0, concat_axis=0, tiled=True)]
    reshape x8 -> x19, local copies, waits for them, and re-layouts: 1.51 us -> 13.7 us  [the longest x2 7.07 us: local(): xg.reshape(8, NSP, 4, 4, 128).transpose(1, 3, 0, 2, 4).reshape(256, 4096)]
    broadcast_in_dim x2 -> x3, local copies, waits for them, and re-layouts: 3.37 us -> 0.16 us  [the longest x2 0.16 us: local(): mx = jnp.where(mine, jnp.maximum(m0, m1), m0)]
    reduce_sum x0 -> x2, other arithmetic: none -> 1.89 us  [the longest x1 1.09 us: local(): out = jnp.sum(oo * fs[:, :, None], axis=0) + own[:, None] * own_values]
    dot_general x2 -> x1, matrix products: 4.62 us -> 4.06 us  [local(): jnp.dot(rows, wo.reshape(4096, 512), preferred_element_type=jnp.float32)]
  transfers between devices with their start and end apart: 5 -> 0, of which waited for: 4 -> 0; matrix products, arithmetic and copies ran while one was open for 10% -> 0% of each run, Pallas kernels for 0% -> 0%
where the time goes in v1:
time: 134 us; the launch traced here: 132 us
  Pallas kernels  100 us (75%)
  local copies, waits for them, and re-layouts  17.8 us (13%)
  other arithmetic  7.63 us (6%)
  matrix products  4.84 us (4%)
    pallas_call x1, Pallas kernels, move(): pl.pallas_call(move_kernel, out_shape=(jax.ShapeDtypeStruct((NSP, 2, 16,...  80.7 us
    pallas_call x1, Pallas kernels, share(): pl.pallas_call(share_kernel, out_shape=(jax.ShapeDtypeStruct((NSP, *o.sha...  19.8 us
    reshape x2, local copies, waits for them, and re-layouts, local(): xg.reshape(8, NSP, 4, 4, 128).transpose(1, 3, 0, 2, 4).reshape(256, 4096)  7.07 us
    dot_general x1, matrix products, local(): jnp.dot(rows, wo.reshape(4096, 512), preferred_element_type=jnp.float32)  4.06 us

profile of v1, /device:TPU:6, one launch (start us, length us, event | category | flops | bytes accessed | tf_op | source)
XLA Modules:
  0.0 131.6 jit_solution(2884477408247978443)
XLA Ops:
  0.7 1.1 reshape.378
  1.8 0.1 copy.21
  1.9 0.8 reshape.381
  2.7 0.8 reshape.380
  3.5 0.1 maximum_bitcast_fusion
  3.7 0.1 reshape.382
  3.8 0.8 pad_maximum_fusion.2
  4.6 80.7 %shard_map.138 = (bf16[64,2,16,256]{3,2,1,0:T(8,128)(2,1)S(1)}, bf16[8,64,16,128]{3,2,1,0:T(8,128)(2,1)S(1)}, f32[64,1,128]{2,1,0:T(1,128)S(1)}, bf16[64,2,32,512]{3,2,1,0:T(8,128)(2,1)S(1)}) custom-call(bf16[64,16,256]{2,1,0:T(8,128)(2,1)S(1)} %bitcast.91, bf16[64,16,256]{2,1,0:T(8,128)(2,1)S(1)} %bitcast.92, bf16[64,16,128]{2,1,0:T(8,128)(2,1)S(1)} %bitcast.93, ...), custom_call_target="tpu_custom_call" | custom-call | tf_op jit(solution)/shard_map/pallas_call | solution.py:218
  85.3 2.6 %copy.70 = bf16[8,64,4,4,128]{4,2,0,3,1:T(4,128)(2,1)} copy(bf16[8,64,4,4,128]{4,3,2,1,0:T(4,128)(2,1)S(1)} %bitcast.90) | data formatting | bytes 4194304 | tf_op jit(solution)/shard_map/reshape | solution.py:330
  87.9 4.5 %reshape.385 = bf16[256,4096]{1,0:T(8,128)(2,1)} reshape(bf16[64,4,8,4,128]{4,3,2,1,0:T(4,128)(2,1)} %bitcast.97) | data formatting | bytes 4194304 | tf_op jit(solution)/shard_map/reshape | solution.py:330
  92.4 4.1 %convolution_convert_fusion = bf16[256,512]{1,0:T(8,128)(2,1)S(1)} fusion(bf16[256,4096]{1,0:T(8,128)(2,1)} %reshape.385, bf16[4096,512]{1,0:T(8,128)(2,1)} %bitcast.96), kind=kOutput, calls=%fused_computation.1 | convolution fusion | flops 1073872896 | bytes 6553600 | tf_op jit(solution)/shard_map/dot_general | solution.py:331
  96.4 0.7 slice_bitcast_fusion.3
  97.1 0.7 reshape.387
  97.8 0.9 slice_bitcast_fusion
  98.7 1.3 pad_maximum_fusion
  100.1 1.0 reshape.388
  101.0 1.0 reshape.390
  102.1 0.1 copy.27
  102.2 0.7 reshape.391
  102.9 0.1 copy.28
  103.0 0.2 copy.43
  103.2 0.2 fusion.33
  103.4 0.2 fusion.31
  103.6 0.2 fusion.10
  103.7 0.3 fusion
  104.0 0.1 copy.29
  104.2 0.1 reshape.397
  104.3 0.2 dynamic-slice_reduce_fusion
  104.5 0.1 copy.44
  104.6 0.1 fusion.24
  104.8 0.2 fusion.29
  105.0 0.2 fusion.22
  105.2 0.2 fusion.3
  105.4 0.7 multiply_add_fusion
  106.1 0.1 broadcast_in_dim.38
  106.2 0.1 reduce_max.33
  106.3 0.1 max.48
  106.4 0.1 mul.115
  106.6 0.6 bitcast_maximum_fusion.m_ref
  107.2 19.8 %shard_map.139 = (f32[64,8,128]{2,1,0:T(8,128)}, f32[64,1,128]{2,1,0:T(1,128)}) custom-call(f32[8,128]{1,0:T(8,128)} %bitcast.106, f32[1,128]{1,0:T(1,128)} %bitcast_maximum_fusion.m_ref), custom_call_target="tpu_custom_call" | custom-call | tf_op jit(solution)/shard_map/pallas_call | solution.py:278
  127.0 0.9 slice.31
  127.9 0.8 slice_reduce_fusion
  128.7 0.1 multiply_reduce_fusion.2
  128.8 0.1 mul.119
  128.9 0.8 multiply_reduce_fusion.1
  129.6 0.1 reduce_sum.58
  129.9 1.1 multiply_reduce_fusion
  131.0 0.6 bitcast_divide_fusion
  (47 shorter events, 0.7 us)
Async XLA Ops:
  0.6 4.0 %copy-start = (bf16[4,256,256]{2,1,0:T(8,128)(2,1)S(1)}, bf16[4,256,256]{2,1,0:T(8,128)(2,1)}, u32[]{:S(2)}) copy-start(bf16[4,256,256]{2,1,0:T(8,128)(2,1)} %param.14) | copy-start | bytes 1572868
  0.6 3.9 %copy-start.1 = (bf16[4,256,256]{2,1,0:T(8,128)(2,1)S(1)}, bf16[4,256,256]{2,1,0:T(8,128)(2,1)}, u32[]{:S(2)}) copy-start(bf16[4,256,256]{2,1,0:T(8,128)(2,1)} %param.15) | copy-start | bytes 1572868
  85.3 2.6 %copy-start.2 = (bf16[64,2,32,512]{3,2,1,0:T(8,128)(2,1)}, bf16[64,2,32,512]{3,2,1,0:T(8,128)(2,1)S(1)}, u32[]{:S(2)}) copy-start(bf16[64,2,32,512]{3,2,1,0:T(8,128)(2,1)S(1)} %get-tuple-element.12) | copy-start | bytes 12582916
  97.1 0.7 copy-start.3
  100.0 2.9 %copy-start.8 = (f32[4,2]{0,1:T(2,128)S(1)}, f32[4,2]{0,1:T(2,128)}, u32[]{:S(2)}) copy-start(f32[4,2]{0,1:T(2,128)} %param.21) | copy-start | bytes 100
  100.0 3.0 %copy-start.7 = (bf16[4,256]{1,0:T(4,128)(2,1)S(1)}, bf16[4,256]{1,0:T(4,128)(2,1)}, u32[]{:S(2)}) copy-start(bf16[4,256]{1,0:T(4,128)(2,1)} %param.18) | copy-start | bytes 6148
  100.0 3.3 %copy-start.6 = (f32[4,2,256]{2,1,0:T(2,128)S(1)}, f32[4,2,256]{2,1,0:T(2,128)}, u32[]{:S(2)}) copy-start(f32[4,2,256]{2,1,0:T(2,128)} %param.16) | copy-start | bytes 24580
  101.0 3.5 %copy-start.4 = (bf16[256,256]{1,0:T(8,128)(2,1)S(1)}, bf16[256,256]{1,0:T(8,128)(2,1)}, u32[]{:S(2)}) copy-start(bf16[256,256]{1,0:T(8,128)(2,1)} %copy-done.3) | copy-start | bytes 393220
  101.0 4.2 %copy-start.5 = (bf16[32,2,8,128]{3,2,1,0:T(8,128)(2,1)S(1)}, bf16[32,2,8,128]{3,2,1,0:T(8,128)(2,1)}, u32[]{:S(2)}) copy-start(bf16[32,2,8,128]{3,2,1,0:T(8,128)(2,1)} %get-tuple-element.26) | copy-start | bytes 393220
  101.0 27.6 %copy-start.9 = (bf16[4,256]{1,0:T(4,128)(2,1)S(1)}, bf16[4,256]{1,0:T(4,128)(2,1)}, u32[]{:S(2)}) copy-start(bf16[4,256]{1,0:T(4,128)(2,1)} %param.19) | copy-start | bytes 6148
  102.0 29.0 %copy-start.10 = (bf16[4,256]{1,0:T(4,128)(2,1)S(1)}, bf16[4,256]{1,0:T(4,128)(2,1)}, u32[]{:S(2)}) copy-start(bf16[4,256]{1,0:T(4,128)(2,1)} %param.20) | copy-start | bytes 6148

commit v2 on v1

v2 whole, which is shorter than its diff:
```python
import functools

import jax
import jax.numpy as jnp
from jax import lax
from jax.experimental import pallas as pl
from jax.experimental.pallas import tpu as pltpu
from jax.sharding import PartitionSpec as P

HEAD_DIM = 128
GROUP = 16
NZ = 8
NY = 8
NSP = 64
NX = 4
MESH = pl.DeviceIdType.MESH
VMEM = pltpu.VMEM

OFFS = (0, -1, 1, -2, 2, -3, 3, -4)


def remote(src, dst, send, recv, sp, tp):
    return pltpu.make_async_remote_copy(
        src_ref=src,
        dst_ref=dst,
        send_sem=send,
        recv_sem=recv,
        device_id=(sp, tp),
        device_id_type=MESH,
    )


def wait_bytes(ref, sem):
    pltpu.make_async_copy(ref, ref, sem).wait()


NEG = -1e37


def dot32(a, b, dims):
    return lax.dot_general(a, b, (dims, ((), ())), preferred_element_type=jnp.float32)


def two_parts(p):
    hi = p.astype(jnp.bfloat16)
    return hi, (p - hi.astype(jnp.float32)).astype(jnp.bfloat16)


def merge(a, b):
    top = jnp.maximum(a[0], b[0])
    fa, fb = jnp.exp(a[0] - top), jnp.exp(b[0] - top)
    return top, a[1] * fa + b[1] * fb, a[2] * fa + b[2] * fb


def swap4(v):
    return pltpu.roll(v, 4, v.ndim - 2)


def step_kernel(
    k_ref,
    v_ref,
    x_ref,
    g_ref,
    w_ref,
    pg_ref,
    q_ref,
    own_k_ref,
    own_v_ref,
    sg_ref,
    ck_ref,
    cv_ref,
    cg_ref,
    out_ref,
    src_ref,
    kv_ref,
    xg_ref,
    rows_ref,
    go_ref,
    wo_ref,
    acc_ref,
    msg_ref,
    got_ref,
    load_sem,
    kv_send,
    kv_recv,
    x_send,
    x_recv,
    g_send,
    g_recv,
    w_send,
    w_recv,
    s_send,
    s_recv,
    p_send,
    p_recv,
):
    sp = lax.axis_index("sp")
    tp = lax.axis_index("tp")
    z, y = sp // NY, lax.rem(sp, NY)
    x, c = tp // 2, lax.rem(tp, 2)
    seq = sp // GROUP
    scale = HEAD_DIM ** (-0.5)

    def at(h, pa, pb):
        pa = lax.rem(pa + 16, 8)
        pb = lax.rem(pb + 16, 8)
        return pa * 8 + pb if h == 0 else pb * 8 + pa

    def peer(d):
        dz, dy = d // NY, lax.rem(d, NY)
        return lax.rem(z + dz, NZ) * NY + lax.rem(y + dy, NY)

    tp_next = lax.rem(x + 1, NX) * 2 + c
    tp_prev = lax.rem(x + NX - 1, NX) * 2 + c
    tp_far = lax.rem(x + 2, NX) * 2 + c
    tp_mate = x * 2 + (1 - c)

    loads = [
        pltpu.make_async_copy(k_ref, src_ref.at[:, 0], load_sem.at[0]),
        pltpu.make_async_copy(v_ref, src_ref.at[:, 1], load_sem.at[1]),
    ]
    for load in loads:
        load.start()

    barrier = pltpu.get_barrier_semaphore()

    def greet(d, carry):
        pl.semaphore_signal(barrier, inc=1, device_id=(peer(d), tp), device_id_type=MESH)
        return carry

    lax.fori_loop(1, NSP, greet, 0)
    for other in (tp_next, tp_prev, tp_mate):
        pl.semaphore_signal(barrier, inc=1, device_id=(sp, other), device_id_type=MESH)
    pl.semaphore_wait(barrier, NSP - 1 + 3)

    pos = ((z, y), (y, z))

    def w_copy(h, i, pa, pb):
        chunk = wo_ref.at[i, h]
        return remote(chunk, chunk, w_send.at[h], w_recv.at[h, i], at(h, pa, pb), tp)

    def w_own(h, pa, pb):
        return remote(w_ref.at[h], wo_ref.at[sp, h], w_send.at[h], w_recv.at[h, sp], at(h, pa, pb), tp)

    def w_wait(h, i):
        wait_bytes(wo_ref.at[i, h], w_recv.at[h, i])

    def second_axis(h, off, dist, step):
        pa, pb = pos[h]
        w_copy(h, at(h, pa + off, pb - dist * step), pa, pb + step).start()

    for h in (0, 1):
        pa, pb = pos[h]
        for step in (1, -1):
            w_own(h, pa + step, pb).start()

    def send_block(d, carry):
        dest = peer(d)
        remote(x_ref.at[dest], xg_ref.at[tp, sp], x_send, x_recv, dest, tp).start()
        remote(g_ref.at[dest], go_ref.at[sp], g_send, g_recv, dest, tp).start()
        return carry

    lax.fori_loop(1, NSP, send_block, 0)

    for h in (0, 1):
        pa, pb = pos[h]
        for step in (1, -1):
            w_own(h, pa, pb + step).start()

    wo_ref[sp] = w_ref[...]
    xg_ref[tp, sp] = x_ref[sp]
    go_ref[sp] = g_ref[sp]
    for load in loads:
        load.wait()
    kv_ref[sp] = src_ref[sp]

    for dist in (1, 2, 3, 4):
        for h in (0, 1):
            pa, pb = pos[h]
            for step in (1, -1):
                if dist == 4 and step == -1:
                    continue
                off = -dist * step
                w_wait(h, at(h, pa + off, pb))
                if dist < (4 if step == 1 else 3):
                    w_copy(h, at(h, pa + off, pb), pa + step, pb).start()
                for side in (1, -1):
                    second_axis(h, off, 0, side)

    def send_past(d, b):
        dest = peer(d)
        remote(src_ref.at[dest], kv_ref.at[sp], kv_send, kv_recv, dest, tp).start()
        return b

    def slab_copy(t, lo, n, k, other):
        ref = xg_ref.at[t, pl.ds(lo, n)]
        return remote(ref, ref, s_send.at[k], s_recv.at[k], sp, other)

    def second_round(dist):
        for off in OFFS:
            for h in (0, 1):
                pa, pb = pos[h]
                for step in (1, -1):
                    w_wait(h, at(h, pa + off, pb - dist * step))
                    if dist < 3 or (step == 1) == (off % 2 == 0):
                        second_axis(h, off, dist, step)

    low = lax.broadcasted_iota(jnp.int32, (1, 8, 128), 1) < 4

    def relay(t):
        def body(n, carry):
            b = xg_ref[t, pl.ds(pl.multiple_of(n * 8, 8), 8)].astype(jnp.float32).reshape(4, 2, 16, 128)
            for half in (0, 1):
                e = b[:, 0, half * 8 : half * 8 + 8]
                o = b[:, 1, half * 8 : half * 8 + 8]
                c0 = jnp.where(low, e, swap4(o)).reshape(32, 128)
                c1 = jnp.where(low, swap4(e), o).reshape(32, 128)
                at_row = pl.ds(pl.multiple_of(n * 32, 32), 32)
                rows_ref[t, at_row, half * 256 : half * 256 + 128] = c0.astype(jnp.bfloat16)
                rows_ref[t, at_row, half * 256 + 128 : half * 256 + 256] = c1.astype(jnp.bfloat16)
            return carry

        lax.fori_loop(0, 8, body, 0)

    second_round(1)

    wait_bytes(xg_ref.at[tp, pl.ds(0, NSP - 1)], x_recv)
    slabs = [slab_copy(tp, 0, NSP, 0, tp_next), slab_copy(tp, 0, NSP, 1, tp_prev), slab_copy(tp, 0, NSP, 2, tp_mate)]
    for s in slabs:
        s.start()
    second_round(2)
    wait_bytes(xg_ref.at[tp_prev], s_recv.at[0])
    wait_bytes(xg_ref.at[tp_next], s_recv.at[1])
    more = [
        slab_copy(tp_prev, 0, NSP // 2, 3, tp_next),
        slab_copy(tp_next, NSP // 2, NSP // 2, 4, tp_prev),
        slab_copy(tp_prev, 0, NSP, 5, tp_mate),
        slab_copy(tp_next, 0, NSP, 6, tp_mate),
    ]
    for s in more:
        s.start()
    second_round(3)
    lax.fori_loop(1, 32, send_past, 0)
    wait_bytes(xg_ref.at[tp_far, pl.ds(0, NSP // 2)], s_recv.at[3])
    wait_bytes(xg_ref.at[tp_far, pl.ds(0, NSP // 2)], s_recv.at[4])
    last = [slab_copy(tp_far, 0, NSP, 7, tp_mate)]
    for s in last:
        s.start()

    row8 = lax.broadcasted_iota(jnp.int32, (8, 256), 0)
    lane8 = lax.broadcasted_iota(jnp.int32, (8, 256), 1)
    row4 = lax.broadcasted_iota(jnp.int32, (4, 128), 0)
    queries = q_ref[...].astype(jnp.float32)

    def heads_apart(qrow):
        return jnp.where(row8 == lane8 // HEAD_DIM, qrow, 0.0).astype(jnp.bfloat16)

    def read(qrow, keys, values, gate0, gate1, own0, own1):
        shift = jnp.where(row8 == 0, own0 - gate0, jnp.where(row8 == 1, own1 - gate1, 0.0))
        scores = dot32(heads_apart(qrow), keys, ((1,), (1,))) * scale + shift
        top = jnp.max(scores, axis=1, keepdims=True)
        p = jnp.exp(scores - top)
        hi, lo = two_parts(p)
        summed = dot32(hi, values, ((1,), (0,))) + dot32(lo, values, ((1,), (0,)))
        return top, jnp.sum(p, axis=1, keepdims=True), summed

    state = [(jnp.full((4, 128), NEG, jnp.float32),) + (jnp.zeros((4, 128), jnp.float32),) * 2 for _ in (0, 1)]

    def place(state, s, part):
        top, den, summed = part
        placed = []
        for h in (0, 1):
            here = row4 == s
            placed.append(
                merge(
                    state[h],
                    (
                        jnp.where(here, top[h : h + 1], NEG),
                        jnp.where(here, den[h : h + 1], 0.0),
                        jnp.where(here, summed[h : h + 1, h * HEAD_DIM : (h + 1) * HEAD_DIM], 0.0),
                    ),
                )
            )
        return placed

    for s in range(4):
        keys = src_ref[s * GROUP : (s + 1) * GROUP, 0].reshape(256, 256)
        values = src_ref[s * GROUP : (s + 1) * GROUP, 1].reshape(256, 256)
        part = read(
            queries[s : s + 1], keys, values, pg_ref[s, 0:1], pg_ref[s, 1:2], sg_ref[s, 0], sg_ref[s, 1]
        )
        state = place(state, s, part)

    for t in (tp, tp_prev, tp_next, tp_far):
        relay(t)

    wait_bytes(go_ref.at[pl.ds(0, NSP - 1)], g_recv)
    gates = go_ref[:, 0, :]

    def spread(width, first):
        n = NSP * width
        source = lax.broadcasted_iota(jnp.int32, (NSP, n), 0)
        column = lax.broadcasted_iota(jnp.int32, (NSP, n), 1)
        picked = lax.dot_general(
            gates,
            (column // width == source).astype(jnp.float32),
            (((0,), (0,)), ((), ())),
            precision=lax.Precision.HIGHEST,
            preferred_element_type=jnp.float32,
        )
        item = lax.broadcasted_iota(jnp.int32, (128, n), 0)
        want = lax.rem(lax.broadcasted_iota(jnp.int32, (128, n), 1), width) + first
        return [jnp.sum(jnp.where(item == want + 20 * h, picked, 0.0), axis=0, keepdims=True) for h in (0, 1)]

    for h, g in enumerate(spread(20, 0)):
        cg_ref[0, h : h + 1, :] = g
    block_gates = spread(4, 16)

    for k in (2, 5, 6, 7):
        wait_bytes(xg_ref.at[tp_mate], s_recv.at[k])
    for t in (tp, tp_prev, tp_next, tp_far):
        relay(t + 1 - 2 * c)
    for off in OFFS:
        for h in (0, 1):
            pa, pb = pos[h]
            w_wait(h, at(h, pa + off, pb + 4))

    acc_ref[...] = jnp.zeros_like(acc_ref)

    def product(t, carry):
        w = wo_ref[pl.ds(pl.multiple_of(t * 8, 8), 8)].reshape(512, 512)
        acc_ref[...] += dot32(rows_ref[t], w, ((1,), (0,)))
        return carry

    lax.fori_loop(0, 8, product, 0)
    both = acc_ref[...].astype(jnp.bfloat16)
    part = read(
        jnp.sum(jnp.where(lax.broadcasted_iota(jnp.int32, (4, 256), 0) == seq, queries, 0.0), axis=0, keepdims=True),
        both[:, :256],
        both[:, 256:],
        block_gates[0],
        block_gates[1],
        sg_ref[seq, 0],
        sg_ref[seq, 1],
    )
    state = place(state, seq, part)

    lane4 = lax.broadcasted_iota(jnp.int32, (4, 128), 1)

    def pack(n, state):
        (m0, l0, o0), (m1, l1, o1) = state
        msg_ref[n, 0] = o0
        msg_ref[n, 1] = o1
        msg_ref[n, 2] = jnp.where(lane4 < 64, jnp.where(lane4 < 32, m0, m1), jnp.where(lane4 < 96, l0, l1))

    def unpack(block):
        ml = block[2]
        cols = [jnp.broadcast_to(ml[:, 32 * n : 32 * n + 1], (4, 128)) for n in range(4)]
        return [(cols[0], cols[2], block[0]), (cols[1], cols[3], block[1])]

    def join(n, state, dest):
        pack(n, state)
        sends = []
        for d in range(1, 8):
            copy = remote(msg_ref.at[n], got_ref.at[n, d], p_send.at[n, d], p_recv.at[n, d], dest(d), tp)
            copy.start()
            sends.append(copy)
        for d in range(1, 8):
            sends[d - 1].wait_recv()
            state = [merge(a, b) for a, b in zip(state, unpack(got_ref[n, d]))]
        return state, sends

    lax.fori_loop(32, 48, send_past, 0)
    state, sends_z = join(0, state, lambda d: lax.rem(z + d, NZ) * NY + y)
    lax.fori_loop(48, 64, send_past, 0)
    state, sends_y = join(1, state, lambda d: z * NY + lax.rem(y + d, NY))

    own_k = own_k_ref[...].astype(jnp.float32)
    own_v = own_v_ref[...].astype(jnp.float32)
    for h in (0, 1):
        cols = slice(h * HEAD_DIM, (h + 1) * HEAD_DIM)
        score = jnp.sum(queries[:, cols] * own_k[:, cols], axis=1, keepdims=True) * scale
        score = jnp.broadcast_to(score, (4, 128))
        _, den, summed = merge(state[h], (score, jnp.ones((4, 128), jnp.float32), own_v[:, cols]))
        out_ref[:, cols] = summed / den

    wait_bytes(kv_ref.at[pl.ds(0, NSP - 1)], kv_recv)

    low2 = lax.broadcasted_iota(jnp.int32, (8, 256), 0) < 4

    def settle(n, carry):
        for a, o_ref in enumerate((ck_ref, cv_ref)):
            pieces = []
            for u in (0, 1):
                pair = 2 * n + u
                blk = acc_ref[pl.ds(pl.multiple_of(pair * 8, 8), 8), a * 256 : (a + 1) * 256]
                pe = kv_ref[2 * pair, a].astype(jnp.float32)
                po = kv_ref[2 * pair + 1, a].astype(jnp.float32)
                r_lo, r_hi = swap4(po[:8]), swap4(po[8:])
                pieces += [
                    pe,
                    jnp.where(low2, blk, r_lo),
                    jnp.where(low2, r_lo, r_hi),
                    jnp.where(low2, r_hi, blk),
                ]
            o_ref[0, pl.ds(pl.multiple_of(n * 80, 80), 80), :] = jnp.concatenate(pieces, axis=0).astype(jnp.bfloat16)
        return carry

    lax.fori_loop(0, 16, settle, 0)

    for s in slabs + more + last + sends_z + sends_y:
        s.wait_send()
    for h in (0, 1):
        wait_bytes(wo_ref.at[pl.ds(0, NSP - 1), 0], w_send.at[h])
    wait_bytes(xg_ref.at[tp, pl.ds(0, NSP - 1)], x_send)
    wait_bytes(go_ref.at[pl.ds(0, NSP - 1)], g_send)
    wait_bytes(kv_ref.at[pl.ds(0, NSP - 1)], kv_send)


def step(*args):
    vm = pl.BlockSpec(memory_space=VMEM)
    dma = pltpu.SemaphoreType.DMA
    bf16, f32 = jnp.bfloat16, jnp.float32
    return pl.pallas_call(
        step_kernel,
        out_shape=(
            jax.ShapeDtypeStruct((1, NSP * 20, 256), bf16),
            jax.ShapeDtypeStruct((1, NSP * 20, 256), bf16),
            jax.ShapeDtypeStruct((1, 2, NSP * 20), f32),
            jax.ShapeDtypeStruct((4, 256), f32),
        ),
        in_specs=[pl.BlockSpec(memory_space=pl.ANY)] * 2 + [vm] * 7 + [pl.BlockSpec(memory_space=pltpu.SMEM)],
        out_specs=(vm,) * 4,
        scratch_shapes=[
            VMEM((NSP, 2, 16, 256), bf16),
            VMEM((NSP, 2, 16, 256), bf16),
            VMEM((8, NSP, 16, 128), bf16),
            VMEM((8, 256, 512), bf16),
            VMEM((NSP, 1, 128), f32),
            VMEM((NSP, 2, 32, 512), bf16),
            VMEM((256, 512), f32),
            VMEM((2, 3, 4, 128), f32),
            VMEM((2, 8, 3, 4, 128), f32),
            dma((2,)),
            dma,
            dma,
            dma,
            dma,
            dma,
            dma,
            dma((2,)),
            dma((2, NSP)),
            dma((8,)),
            dma((8,)),
            dma((2, 8)),
            dma((2, 8)),
        ],
        compiler_params=pltpu.CompilerParams(
            collective_id=0, has_side_effects=True, vmem_limit_bytes=40 * 1024 * 1024
        ),
    )(*args)


def local(
    block_input,
    key_weight,
    value_weight,
    earlier_keys,
    past_values,
    past_gates,
    block_gates,
    step_query,
    step_key,
    step_value,
    step_gate,
):
    seqs = block_input.shape[0]
    heads = 2
    xb = block_input.reshape(seqs, GROUP, 4, 4, 128).transpose(0, 1, 3, 2, 4).reshape(NSP, 16, 128)
    past_parts = past_gates.reshape(seqs, heads, GROUP, 16)
    block_parts = block_gates.reshape(seqs, heads, GROUP, 4)
    gates = jnp.concatenate([past_parts, block_parts], axis=3).transpose(0, 2, 1, 3).reshape(NSP, 1, 40)
    gates = jnp.pad(gates, ((0, 0), (0, 0), (0, 88)))
    w = jnp.concatenate([key_weight, value_weight], axis=1).reshape(2, 32, 512)
    return step(
        earlier_keys.reshape(NSP, 16, 256),
        past_values.reshape(NSP, 16, 256),
        xb,
        gates,
        w,
        past_gates,
        step_query,
        step_key,
        step_value,
        step_gate,
    )


def solution(mesh):
    in_specs = (
        P(None, "sp", "tp"),
        P("sp", "tp"),
        P("sp", "tp"),
        P(None, "sp", "tp"),
        P(None, "sp", "tp"),
        P(None, "tp", "sp"),
        P(None, "tp", "sp"),
        P(None, "tp"),
        P(None, "tp"),
        P(None, "tp"),
        P(None, "tp"),
    )
    out_specs = (P("sp", None, "tp"), P("sp", None, "tp"), P("sp", "tp", None), P(None, "tp"))
    return jax.shard_map(local, mesh=mesh, in_specs=in_specs, out_specs=out_specs, check_vma=False)
```

time: 134 us -> 107 us (0.80); the launches traced: 132 us -> 107 us
  local copies, waits for them, and re-layouts: 17.8 us -> 6.43 us
  other arithmetic: 7.63 us -> 0.93 us
  matrix products: 4.84 us -> 0 us
    reshape x12 -> x0, local copies, waits for them, and re-layouts: 10.8 us -> none  [the longest x2 7.07 us: local(): xg.reshape(8, NSP, 4, 4, 128).transpose(1, 3, 0, 2, 4).reshape(256, 4096)]
    unnamed x25 -> x23, local copies, waits for them, and re-layouts: 0.89 us -> 5.89 us
    dot_general x5 -> x0, matrix products: 4.84 us -> none  [the longest x1 4.06 us: local(): jnp.dot(rows, wo.reshape(4096, 512), preferred_element_type=jnp.float32)]
    reduce_sum x5 -> x0, other arithmetic: 2.33 us -> none  [the longest x1 1.09 us: local(): out = jnp.sum(oo * fs[:, :, None], axis=0) + own[:, None] * own_values]
    concatenate x2 -> x0, other arithmetic: 1.84 us -> none  [the longest x1 1.28 us: local(): jnp.concatenate([kv[:, 0], kb.reshape(NSP, 4, 256)], axis=1)]
    pallas_call x2 -> x1, Pallas kernels: 100 us -> 98.8 us  [step(): pl.pallas_call(step_kernel, out_shape=(jax.ShapeDtypeStruct((1, NSP * 20,...]
where the time goes in v2:
time: 107 us
  Pallas kernels  98.8 us (92%)
  local copies, waits for them, and re-layouts  6.43 us (6%)
    pallas_call x1, Pallas kernels, step(): pl.pallas_call(step_kernel, out_shape=(jax.ShapeDtypeStruct((1, NSP * 20,...  98.8 us
    unnamed x23, local copies, waits for them, and re-layouts  5.89 us

profile of v2, /device:TPU:6, one launch (start us, length us, event | category | flops | bytes accessed | tf_op | source)
XLA Modules:
  0.0 106.9 jit_solution(10252184086186462979)
XLA Ops:
  0.6 0.0 copy-start.8
  0.6 0.7 copy-done.8
  1.3 0.1 copy.23.sg_ref
  1.4 0.0 copy-start.7
  1.4 0.8 pad_maximum_fusion
  2.2 0.0 copy-done.7
  2.2 0.1 reshape.37
  2.3 0.0 copy-start.2
  2.4 0.6 copy-done.2
  3.0 0.1 reshape.36
  3.1 0.0 copy-start.6
  3.1 0.1 maximum_bitcast_fusion
  3.3 0.1 reshape.38
  3.4 0.0 copy-start.3
  3.4 0.0 copy-start.4
  3.4 0.0 copy-start.5
  3.4 0.6 copy-done.6
  4.0 0.0 copy-start
  4.0 0.0 copy-start.1
  4.0 0.1 reshape.34
  4.1 0.1 copy.19
  4.2 0.0 copy-done.3
  4.2 0.0 copy-done.4
  4.2 0.0 copy-done.5
  4.3 0.8 copy-done
  5.1 0.2 copy-done.1
  5.2 98.8 %shard_map.138 = (bf16[1,1280,256]{2,1,0:T(8,128)(2,1)S(1)}, bf16[1,1280,256]{2,1,0:T(8,128)(2,1)S(1)}, f32[1,2,1280]{2,1,0:T(2,128)S(1)}, f32[4,256]{1,0:T(4,128)S(1)}) custom-call(bf16[64,16,256]{2,1,0:T(8,128)(2,1)S(1)} %bitcast.10, bf16[64,16,256]{2,1,0:T(8,128)(2,1)S(1)} %bitcast.11, bf16[64,16,128]{2,1,0:T(8,128)(2,1)S(1)} %bitcast.9, ...), custom_call_target="tpu_custom_call" | custom-call | tf_op jit(solution)/shard_map/pallas_call | solution.py:424
  104.1 0.8 copy.28
  104.9 0.8 copy.29
  105.7 0.6 copy.30
  106.3 0.6 copy.31
  (3 shorter events, 0.1 us)
Async XLA Ops:
  0.6 0.7 copy-start.8
  1.4 0.8 copy-start.7
  2.3 0.7 copy-start.2
  3.1 1.0 copy-start.6
  3.4 0.8 copy-start.3
  3.4 0.8 copy-start.4
  3.4 0.9 copy-start.5
  4.0 1.0 copy-start
  4.0 1.2 %copy-start.1 = (bf16[4,256,256]{2,1,0:T(8,128)(2,1)S(1)}, bf16[4,256,256]{2,1,0:T(8,128)(2,1)}, u32[]{:S(2)}) copy-start(bf16[4,256,256]{2,1,0:T(8,128)(2,1)} %param.15) | copy-start | bytes 1572868

commit v3 on v2

v3 whole, which is shorter than its diff:
```python
import functools

import jax
import jax.numpy as jnp
from jax import lax
from jax.experimental import pallas as pl
from jax.experimental.pallas import tpu as pltpu
from jax.sharding import PartitionSpec as P

HEAD_DIM = 128
GROUP = 16
NZ = 8
NY = 8
NSP = 64
NX = 4
MESH = pl.DeviceIdType.MESH
VMEM = pltpu.VMEM

PAST_AT = (8, 4, 0, 0, 12, 12, 27)
OFFS = (0, -1, 1, -2, 2, -3, 3, -4)


def remote(src, dst, send, recv, sp, tp):
    return pltpu.make_async_remote_copy(
        src_ref=src,
        dst_ref=dst,
        send_sem=send,
        recv_sem=recv,
        device_id=(sp, tp),
        device_id_type=MESH,
    )


def wait_bytes(ref, sem):
    pltpu.make_async_copy(ref, ref, sem).wait()


NEG = -1e37


def dot32(a, b, dims):
    return lax.dot_general(a, b, (dims, ((), ())), preferred_element_type=jnp.float32)


def two_parts(p):
    hi = p.astype(jnp.bfloat16)
    return hi, (p - hi.astype(jnp.float32)).astype(jnp.bfloat16)


def merge(a, b):
    top = jnp.maximum(a[0], b[0])
    fa, fb = jnp.exp(a[0] - top), jnp.exp(b[0] - top)
    return top, a[1] * fa + b[1] * fb, a[2] * fa + b[2] * fb


def swap4(v):
    return pltpu.roll(v, 4, v.ndim - 2)


def step_kernel(
    k_hbm,
    v_hbm,
    x_hbm,
    kw_hbm,
    vw_hbm,
    pg_hbm,
    bg_hbm,
    q_hbm,
    own_k_hbm,
    own_v_hbm,
    sg_ref,
    kv_ref,
    kvb_ref,
    cg_ref,
    out_ref,
    src_ref,
    in_ref,
    pg_ref,
    bg_ref,
    q_ref,
    own_k_ref,
    own_v_ref,
    x_ref,
    g_ref,
    xg_ref,
    rows_ref,
    go_ref,
    wo_ref,
    acc_ref,
    msg_ref,
    got_ref,
    part_ref,
    parts_ref,
    load_sem,
    kv_send,
    kv_recv,
    x_send,
    x_recv,
    g_send,
    g_recv,
    w_send,
    w_recv,
    s_send,
    s_recv,
    p_send,
    p_recv,
    b_send,
    b_recv,
    keep_sem,
    near,
    rows_in,
):
    sp = lax.axis_index("sp")
    tp = lax.axis_index("tp")
    z, y = sp // NY, lax.rem(sp, NY)
    x, c = tp // 2, lax.rem(tp, 2)
    seq = sp // GROUP
    scale = HEAD_DIM ** (-0.5)

    def at(h, pa, pb):
        pa = lax.rem(pa + 16, 8)
        pb = lax.rem(pb + 16, 8)
        return pa * 8 + pb if h == 0 else pb * 8 + pa

    def peer(d):
        d = lax.rem(d * 45, NSP)
        dz, dy = d // NY, lax.rem(d, NY)
        return lax.rem(z + dz, NZ) * NY + lax.rem(y + dy, NY)

    tp_next = lax.rem(x + 1, NX) * 2 + c
    tp_prev = lax.rem(x + NX - 1, NX) * 2 + c
    tp_far = lax.rem(x + 2, NX) * 2 + c
    tp_mate = x * 2 + (1 - c)

    moves = (
        (k_hbm, src_ref.at[:, 0]),
        (v_hbm, src_ref.at[:, 1]),
        (kw_hbm, wo_ref.at[sp, 0]),
        (vw_hbm, wo_ref.at[sp, 1]),
        (x_hbm, in_ref),
        (pg_hbm, pg_ref),
        (bg_hbm, bg_ref),
        (q_hbm, q_ref),
        (own_k_hbm, own_k_ref),
        (own_v_hbm, own_v_ref),
    )
    loads = [pltpu.make_async_copy(a, b, load_sem.at[n]) for n, (a, b) in enumerate(moves)]
    for load in loads:
        load.start()

    barrier = pltpu.get_barrier_semaphore()

    z_next, z_prev = at(0, z + 1, y), at(0, z - 1, y)
    y_next, y_prev = at(0, z, y + 1), at(0, z, y - 1)
    for other in (z_next, z_prev, y_next, y_prev):
        pl.semaphore_signal(barrier, inc=1, device_id=(other, tp), device_id_type=MESH)
    for other in (tp_next, tp_prev, tp_mate):
        pl.semaphore_signal(barrier, inc=1, device_id=(sp, other), device_id_type=MESH)

    for load in loads:
        load.wait()

    low = lax.broadcasted_iota(jnp.int32, (1, 8, 128), 1) < 4

    def split(n, carry):
        at_row = pl.ds(pl.multiple_of(n * 32, 32), 32)
        halves = []
        for half in (0, 1):
            c0 = in_ref[at_row, half * 256 : half * 256 + 128].astype(jnp.float32).reshape(4, 8, 128)
            c1 = in_ref[at_row, half * 256 + 128 : half * 256 + 256].astype(jnp.float32).reshape(4, 8, 128)
            halves.append((jnp.where(low, c0, swap4(c1)), jnp.where(low, swap4(c0), c1)))
        even = jnp.concatenate([halves[0][0], halves[1][0]], axis=1)
        odd = jnp.concatenate([halves[0][1], halves[1][1]], axis=1)
        both = jnp.stack([even, odd], axis=1).reshape(8, 16, 128)
        x_ref[pl.ds(pl.multiple_of(n * 8, 8), 8)] = both.astype(jnp.bfloat16)
        return carry

    lax.fori_loop(0, 8, split, 0)

    for s in range(4):
        row = jnp.zeros((GROUP, 128), jnp.float32)
        for h in (0, 1):
            for ref, width, first in ((pg_ref, 16, 0), (bg_ref, 4, 16)):
                n = GROUP * width
                mine = lax.broadcasted_iota(jnp.int32, (GROUP, n), 1) // width
                mine = mine == lax.broadcasted_iota(jnp.int32, (GROUP, n), 0)
                item = lax.rem(lax.broadcasted_iota(jnp.int32, (n, 128), 0), width) + 20 * h + first
                row += lax.dot_general(
                    jnp.where(mine, ref[s, h : h + 1], 0.0),
                    (item == lax.broadcasted_iota(jnp.int32, (n, 128), 1)).astype(jnp.float32),
                    (((1,), (0,)), ((), ())),
                    precision=lax.Precision.HIGHEST,
                    preferred_element_type=jnp.float32,
                )
        g_ref[s * GROUP : (s + 1) * GROUP, 0, :] = row

    row8 = lax.broadcasted_iota(jnp.int32, (8, 256), 0)
    lane8 = lax.broadcasted_iota(jnp.int32, (8, 256), 1)
    row4 = lax.broadcasted_iota(jnp.int32, (4, 128), 0)
    queries = q_ref[...].astype(jnp.float32)

    def heads_apart(qrow):
        return jnp.where(row8 == lane8 // HEAD_DIM, qrow, 0.0).astype(jnp.bfloat16)

    def read(qrow, keys, values, gate0, gate1, own0, own1):
        shift = jnp.where(row8 == 0, own0 - gate0, jnp.where(row8 == 1, own1 - gate1, 0.0))
        scores = dot32(heads_apart(qrow), keys, ((1,), (1,))) * scale + shift
        top = jnp.max(scores, axis=1, keepdims=True)
        p = jnp.exp(scores - top)
        hi, lo = two_parts(p)
        summed = dot32(hi, values, ((1,), (0,))) + dot32(lo, values, ((1,), (0,)))
        return top, jnp.sum(p, axis=1, keepdims=True), summed

    state = [(jnp.full((4, 128), NEG, jnp.float32),) + (jnp.zeros((4, 128), jnp.float32),) * 2 for _ in (0, 1)]

    def join_row(state, s, top, den, summed):
        here = row4 == s
        return merge(state, (jnp.where(here, top, NEG), jnp.where(here, den, 0.0), jnp.where(here, summed, 0.0)))

    for s in range(4):
        keys = src_ref[s * GROUP : (s + 1) * GROUP, 0].reshape(256, 256)
        values = src_ref[s * GROUP : (s + 1) * GROUP, 1].reshape(256, 256)
        part = read(
            queries[s : s + 1], keys, values, pg_ref[s, 0:1], pg_ref[s, 1:2], sg_ref[0, s], sg_ref[1, s]
        )
        for h in (0, 1):
            cols = slice(h * HEAD_DIM, (h + 1) * HEAD_DIM)
            state[h] = join_row(state[h], s, *(a[h : h + 1] for a in part[:2]), part[2][h : h + 1, cols])

    lane4 = lax.broadcasted_iota(jnp.int32, (4, 128), 1)

    def pack(n, state):
        (m0, l0, o0), (m1, l1, o1) = state
        msg_ref[n, 0] = o0
        msg_ref[n, 1] = o1
        msg_ref[n, 2] = jnp.where(lane4 < 64, jnp.where(lane4 < 32, m0, m1), jnp.where(lane4 < 96, l0, l1))

    def unpack(block):
        ml = block[2]
        cols = [jnp.broadcast_to(ml[:, 32 * n : 32 * n + 1], (4, 128)) for n in range(4)]
        return [(cols[0], cols[2], block[0]), (cols[1], cols[3], block[1])]

    def exchange(n, dest):
        copies = [
            remote(msg_ref.at[n], got_ref.at[n, d], p_send.at[n, d], p_recv.at[n, d], dest(d), tp)
            for d in range(1, 8)
        ]
        for copy in copies:
            copy.start()
        return copies

    def gather(n, copies, state):
        for d in range(1, 8):
            copies[d - 1].wait_recv()
            state = [merge(a, b) for a, b in zip(state, unpack(got_ref[n, d]))]
        return state

    pack(0, state)
    pl.semaphore_wait(barrier, 7)

    pos = ((z, y), (y, z))

    def w_copy(h, i, pa, pb):
        chunk = wo_ref.at[i, h]
        return remote(chunk, chunk, w_send.at[h], w_recv.at[h, i], at(h, pa, pb), tp)

    def w_own(h, pa, pb):
        return w_copy(h, sp, pa, pb)

    def w_wait(h, i):
        wait_bytes(wo_ref.at[i, h], w_recv.at[h, i])

    def second_axis(h, off, dist, step):
        pa, pb = pos[h]
        w_copy(h, at(h, pa + off, pb - dist * step), pa, pb + step).start()

    for h in (0, 1):
        pa, pb = pos[h]
        for step in (1, -1):
            w_own(h, pa + step, pb).start()
    for h in (0, 1):
        pa, pb = pos[h]
        for step in (1, -1):
            w_own(h, pa, pb + step).start()

    def pass_word():
        for n, other in enumerate((z_next, z_prev, y_next, y_prev)):
            pl.semaphore_signal(near.at[n], inc=1, device_id=(other, tp), device_id_type=MESH)
        for n in range(4):
            pl.semaphore_wait(near.at[n], 1)

    def weights_in(dist):
        for h in (0, 1):
            pa, pb = pos[h]
            for step in (1, -1):
                if dist == 4 and step == -1:
                    continue
                off = -dist * step
                w_wait(h, at(h, pa + off, pb))
                if dist < (4 if step == 1 else 3):
                    w_copy(h, at(h, pa + off, pb), pa + step, pb).start()
                for side in (1, -1):
                    second_axis(h, off, 0, side)

    pass_word()
    pass_word()
    weights_in(1)
    pass_word()
    for d in range(1, 8):
        other = at(0, z, y + d)
        pl.semaphore_signal(rows_in, inc=1, device_id=(other, tp), device_id_type=MESH)
    weights_in(2)
    pl.semaphore_wait(rows_in, 7)

    sends_z = exchange(0, lambda d: lax.rem(z + d, NZ) * NY + y)

    def send_block(d, carry):
        dest = peer(d)
        remote(x_ref.at[dest], xg_ref.at[tp, sp], x_send, x_recv, dest, tp).start()
        remote(g_ref.at[dest], go_ref.at[sp], g_send, g_recv, dest, tp).start()
        return carry

    lax.fori_loop(1, NSP, send_block, 0)

    def send_past(d, b):
        dest = peer(d)
        remote(src_ref.at[dest], kv_ref.at[sp], kv_send, kv_recv, dest, tp).start()
        return b

    def stage(n):
        first = 1 + sum(PAST_AT[:n])
        if PAST_AT[n]:
            lax.fori_loop(first, first + PAST_AT[n], send_past, 0)

    xg_ref[tp, sp] = x_ref[sp]
    go_ref[sp] = g_ref[sp]
    kept = pltpu.make_async_copy(src_ref.at[sp], kv_ref.at[sp], keep_sem)
    kept.start()
    stage(0)

    weights_in(3)
    weights_in(4)

    def slab_copy(t, lo, n, k, other):
        ref = xg_ref.at[t, pl.ds(lo, n)]
        return remote(ref, ref, s_send.at[k], s_recv.at[k], sp, other)

    def second_round(dist):
        for off in OFFS:
            for h in (0, 1):
                pa, pb = pos[h]
                for step in (1, -1):
                    w_wait(h, at(h, pa + off, pb - dist * step))
                    if dist < 3 or (step == 1) == (off % 2 == 0):
                        second_axis(h, off, dist, step)


    def relay(t):
        def body(n, carry):
            b = xg_ref[t, pl.ds(pl.multiple_of(n * 8, 8), 8)].astype(jnp.float32).reshape(4, 2, 16, 128)
            for half in (0, 1):
                e = b[:, 0, half * 8 : half * 8 + 8]
                o = b[:, 1, half * 8 : half * 8 + 8]
                c0 = jnp.where(low, e, swap4(o)).reshape(32, 128)
                c1 = jnp.where(low, swap4(e), o).reshape(32, 128)
                at_row = pl.ds(pl.multiple_of(n * 32, 32), 32)
                rows_ref[t, at_row, half * 256 : half * 256 + 128] = c0.astype(jnp.bfloat16)
                rows_ref[t, at_row, half * 256 + 128 : half * 256 + 256] = c1.astype(jnp.bfloat16)
            return carry

        lax.fori_loop(0, 8, body, 0)

    stage(1)
    state = gather(0, sends_z, state)
    pack(1, state)
    second_round(1)
    stage(2)
    sends_y = exchange(1, lambda d: z * NY + lax.rem(y + d, NY))

    wait_bytes(xg_ref.at[tp, pl.ds(0, NSP - 1)], x_recv)
    slabs = [slab_copy(tp, 0, NSP, 0, tp_next), slab_copy(tp, 0, NSP, 1, tp_prev), slab_copy(tp, 0, NSP, 2, tp_mate)]
    for s in slabs:
        s.start()
    second_round(2)
    stage(3)
    wait_bytes(xg_ref.at[tp_prev], s_recv.at[0])
    wait_bytes(xg_ref.at[tp_next], s_recv.at[1])
    more = [
        slab_copy(tp_prev, 0, NSP // 2, 3, tp_next),
        slab_copy(tp_next, NSP // 2, NSP // 2, 4, tp_prev),
        slab_copy(tp_prev, 0, NSP, 5, tp_mate),
        slab_copy(tp_next, 0, NSP, 6, tp_mate),
    ]
    for s in more:
        s.start()
    second_round(3)
    stage(4)
    state = gather(1, sends_y, state)
    wait_bytes(xg_ref.at[tp_far, pl.ds(0, NSP // 2)], s_recv.at[3])
    wait_bytes(xg_ref.at[tp_far, pl.ds(0, NSP // 2)], s_recv.at[4])
    last = [slab_copy(tp_far, 0, NSP, 7, tp_mate)]
    for s in last:
        s.start()

    for t in (tp, tp_prev, tp_next, tp_far):
        relay(t)

    wait_bytes(go_ref.at[pl.ds(0, NSP - 1)], g_recv)
    gates = go_ref[:, 0, :]

    def spread(width, first):
        n = NSP * width
        source = lax.broadcasted_iota(jnp.int32, (NSP, n), 0)
        column = lax.broadcasted_iota(jnp.int32, (NSP, n), 1)
        picked = lax.dot_general(
            gates,
            (column // width == source).astype(jnp.float32),
            (((0,), (0,)), ((), ())),
            precision=lax.Precision.HIGHEST,
            preferred_element_type=jnp.float32,
        )
        item = lax.broadcasted_iota(jnp.int32, (128, n), 0)
        want = lax.rem(lax.broadcasted_iota(jnp.int32, (128, n), 1), width) + first
        return [jnp.sum(jnp.where(item == want + 20 * h, picked, 0.0), axis=0, keepdims=True) for h in (0, 1)]

    for h, g in enumerate(spread(20, 0)):
        cg_ref[h : h + 1, :] = g
    block_gates = spread(4, 16)

    for k in (2, 5, 6, 7):
        wait_bytes(xg_ref.at[tp_mate], s_recv.at[k])
    for t in (tp, tp_prev, tp_next, tp_far):
        relay(t + 1 - 2 * c)
    for off in OFFS:
        for h in (0, 1):
            pa, pb = pos[h]
            w_wait(h, at(h, pa + off, pb + 4))

    stage(5)
    acc_ref[...] = jnp.zeros_like(acc_ref)

    def product(t, carry):
        for h in (0, 1):
            w = wo_ref[pl.ds(pl.multiple_of(t * 8, 8), 8), h].reshape(512, 256)
            acc_ref[:, h * 256 : (h + 1) * 256] += dot32(rows_ref[t], w, ((1,), (0,)))
        return carry

    lax.fori_loop(0, 8, product, 0)
    both = acc_ref[...].astype(jnp.bfloat16)
    kvb_ref[...] = both
    part = read(
        jnp.sum(jnp.where(lax.broadcasted_iota(jnp.int32, (4, 256), 0) == seq, queries, 0.0), axis=0, keepdims=True),
        both[:, :256],
        both[:, 256:],
        block_gates[0],
        block_gates[1],
        sg_ref[0, seq],
        sg_ref[1, seq],
    )
    top, den, summed = part
    lane1 = lax.broadcasted_iota(jnp.int32, (1, 128), 1)
    ml = jnp.where(
        lane1 < 64,
        jnp.where(lane1 < 32, top[0:1], top[1:2]),
        jnp.where(lane1 < 96, den[0:1], den[1:2]),
    )
    part_ref[0] = jnp.concatenate([summed[0:1, :128], summed[1:2, 128:], ml, ml], axis=0)

    def send_part(d, carry):
        remote(part_ref.at[0], parts_ref.at[sp], b_send, b_recv, peer(d), tp).start()
        return carry

    lax.fori_loop(1, NSP, send_part, 0)
    parts_ref[sp] = part_ref[0]
    stage(6)
    wait_bytes(parts_ref.at[pl.ds(0, NSP - 1)], b_recv)
    for s in range(4):
        group = pl.ds(s * GROUP, GROUP)
        marks = parts_ref[group, 2, :]
        for h in (0, 1):
            m = marks[:, 32 * h : 32 * h + 1]
            top = jnp.max(m, axis=0, keepdims=True)
            f = jnp.exp(m - top)
            den = jnp.sum(marks[:, 64 + 32 * h : 65 + 32 * h] * f, axis=0, keepdims=True)
            summed = jnp.sum(parts_ref[group, h, :] * f, axis=0, keepdims=True)
            state[h] = join_row(state[h], s, top, den, summed)

    own_k = own_k_ref[...].astype(jnp.float32)
    own_v = own_v_ref[...].astype(jnp.float32)
    for h in (0, 1):
        cols = slice(h * HEAD_DIM, (h + 1) * HEAD_DIM)
        score = jnp.sum(queries[:, cols] * own_k[:, cols], axis=1, keepdims=True) * scale
        score = jnp.broadcast_to(score, (4, 128))
        _, den, summed = merge(state[h], (score, jnp.ones((4, 128), jnp.float32), own_v[:, cols]))
        out_ref[:, cols] = summed / den

    for s in slabs + more + last + sends_z + sends_y:
        s.wait_send()
    for h in (0, 1):
        wait_bytes(wo_ref.at[pl.ds(0, NSP - 1), 0], w_send.at[h])
    wait_bytes(xg_ref.at[tp, pl.ds(0, NSP - 1)], x_send)
    wait_bytes(go_ref.at[pl.ds(0, NSP - 1)], g_send)
    wait_bytes(src_ref.at[pl.ds(0, NSP - 1)], kv_send)
    wait_bytes(src_ref.at[pl.ds(0, NSP - 1)], kv_recv)
    kept.wait()
    wait_bytes(parts_ref.at[pl.ds(0, NSP - 1)], b_send)


def step(*args):
    vm = pl.BlockSpec(memory_space=VMEM)
    dma = pltpu.SemaphoreType.DMA
    bf16, f32 = jnp.bfloat16, jnp.float32
    return pl.pallas_call(
        step_kernel,
        out_shape=(
            jax.ShapeDtypeStruct((NSP, 2, 16, 256), bf16),
            jax.ShapeDtypeStruct((256, 512), bf16),
            jax.ShapeDtypeStruct((2, NSP * 20), f32),
            jax.ShapeDtypeStruct((4, 256), f32),
        ),
        in_specs=[pl.BlockSpec(memory_space=pl.ANY)] * 10 + [pl.BlockSpec(memory_space=pltpu.SMEM)],
        out_specs=(pl.BlockSpec(memory_space=pl.ANY), vm, vm, vm),
        scratch_shapes=[
            VMEM((NSP, 2, 16, 256), bf16),
            VMEM((256, 512), bf16),
            VMEM((4, 2, 256), f32),
            VMEM((4, 2, 64), f32),
            VMEM((4, 256), bf16),
            VMEM((4, 256), bf16),
            VMEM((4, 256), bf16),
            VMEM((NSP, 16, 128), bf16),
            VMEM((NSP, 1, 128), f32),
            VMEM((8, NSP, 16, 128), bf16),
            VMEM((8, 256, 512), bf16),
            VMEM((NSP, 1, 128), f32),
            VMEM((NSP, 2, 64, 256), bf16),
            VMEM((256, 512), f32),
            VMEM((2, 3, 4, 128), f32),
            VMEM((2, 8, 3, 4, 128), f32),
            VMEM((1, 4, 128), f32),
            VMEM((NSP, 4, 128), f32),
            dma((10,)),
            dma,
            dma,
            dma,
            dma,
            dma,
            dma,
            dma((2,)),
            dma((2, NSP)),
            dma((8,)),
            dma((8,)),
            dma((2, 8)),
            dma((2, 8)),
            dma,
            dma,
            dma,
            pltpu.SemaphoreType.REGULAR((4,)),
            pltpu.SemaphoreType.REGULAR,
        ],
        compiler_params=pltpu.CompilerParams(
            collective_id=0, has_side_effects=True, vmem_limit_bytes=60 * 1024 * 1024
        ),
    )(*args)


def settle_kernel(kv_ref, kvb_ref, g_ref, o_ref, ck_ref, cv_ref, cg_ref, out_ref):
    low = lax.broadcasted_iota(jnp.int32, (8, 256), 0) < 4
    cg_ref[0] = g_ref[...]
    out_ref[...] = o_ref[...]

    def settle(n, carry):
        block = kvb_ref[pl.ds(pl.multiple_of(n * 16, 16), 16), :].astype(jnp.float32)
        for a, to_ref in enumerate((ck_ref, cv_ref)):
            pieces = []
            for u in (0, 1):
                pair = 2 * n + u
                blk = block[8 * u : 8 * u + 8, a * 256 : (a + 1) * 256]
                pe = kv_ref[2 * pair, a].astype(jnp.float32)
                po = kv_ref[2 * pair + 1, a].astype(jnp.float32)
                r_lo, r_hi = swap4(po[:8]), swap4(po[8:])
                pieces += [
                    pe,
                    jnp.where(low, blk, r_lo),
                    jnp.where(low, r_lo, r_hi),
                    jnp.where(low, r_hi, blk),
                ]
            rows = jnp.concatenate(pieces, axis=0).astype(jnp.bfloat16)
            to_ref[0, pl.ds(pl.multiple_of(n * 80, 80), 80), :] = rows
        return carry

    lax.fori_loop(0, kv_ref.shape[0] // 4, settle, 0, unroll=2)


def settled(kv, kvb, g, o):
    steps = 4
    bf16, f32 = jnp.bfloat16, jnp.float32
    rows = NSP * 20 // steps
    return pl.pallas_call(
        settle_kernel,
        grid=(steps,),
        out_shape=(
            jax.ShapeDtypeStruct((1, NSP * 20, 256), bf16),
            jax.ShapeDtypeStruct((1, NSP * 20, 256), bf16),
            jax.ShapeDtypeStruct((1, 2, NSP * 20), f32),
            jax.ShapeDtypeStruct((4, 256), f32),
        ),
        in_specs=[
            pl.BlockSpec((NSP // steps, 2, 16, 256), lambda n: (n, 0, 0, 0)),
            pl.BlockSpec((256 // steps, 512), lambda n: (n, 0)),
            pl.BlockSpec((2, NSP * 20), lambda n: (0, 0)),
            pl.BlockSpec((4, 256), lambda n: (0, 0)),
        ],
        out_specs=(
            pl.BlockSpec((1, rows, 256), lambda n: (0, n, 0)),
            pl.BlockSpec((1, rows, 256), lambda n: (0, n, 0)),
            pl.BlockSpec((1, 2, NSP * 20), lambda n: (0, 0, 0)),
            pl.BlockSpec((4, 256), lambda n: (0, 0)),
        ),
        compiler_params=pltpu.CompilerParams(vmem_limit_bytes=60 * 1024 * 1024),
    )(kv, kvb, g, o)


def local(
    block_input,
    key_weight,
    value_weight,
    earlier_keys,
    past_values,
    past_gates,
    block_gates,
    step_query,
    step_key,
    step_value,
    step_gate,
):
    moved = step(
        earlier_keys.reshape(NSP, 16, 256),
        past_values.reshape(NSP, 16, 256),
        block_input.reshape(256, 512),
        key_weight,
        value_weight,
        past_gates,
        block_gates,
        step_query,
        step_key,
        step_value,
        step_gate.T,
    )
    return settled(*moved)


def solution(mesh):
    in_specs = (
        P(None, "sp", "tp"),
        P("sp", "tp"),
        P("sp", "tp"),
        P(None, "sp", "tp"),
        P(None, "sp", "tp"),
        P(None, "tp", "sp"),
        P(None, "tp", "sp"),
        P(None, "tp"),
        P(None, "tp"),
        P(None, "tp"),
        P(None, "tp"),
    )
    out_specs = (P("sp", None, "tp"), P("sp", None, "tp"), P("sp", "tp", None), P(None, "tp"))
    return jax.shard_map(local, mesh=mesh, in_specs=in_specs, out_specs=out_specs, check_vma=False)
```

time: 107 us -> 84.5 us (0.79)
  the two profiles are of different devices: /device:TPU:6 before, /device:TPU:1 now
where the time goes in v3:
time: 84.5 us; the launch traced here: 84.3 us
  Pallas kernels  83.7 us (99%)
    pallas_call x1, Pallas kernels, step(): pl.pallas_call(step_kernel, out_shape=(jax.ShapeDtypeStruct((NSP, 2, 16,...  80.2 us
    pallas_call x1, Pallas kernels, settled(): pl.pallas_call(settle_kernel, grid=(steps,), out_shape=(jax.ShapeDtypeStr...  3.5 us

profile of v3, /device:TPU:1, one launch (start us, length us, event | category | flops | bytes accessed | tf_op | source)
XLA Modules:
  0.0 84.3 jit_solution(11126861255150511345)
XLA Ops:
  0.6 80.2 %shard_map.138 = (bf16[64,2,16,256]{3,2,1,0:T(8,128)(2,1)}, bf16[256,512]{1,0:T(8,128)(2,1)}, f32[2,1280]{1,0:T(2,128)}, f32[4,256]{1,0:T(4,128)}) custom-call(bf16[64,16,256]{2,1,0:T(8,128)(2,1)} %bitcast.4, bf16[64,16,256]{2,1,0:T(8,128)(2,1)} %bitcast.5, bf16[256,512]{1,0:T(8,128)(2,1)} %bitcast.6, bf16[64,256]{1,0:T(8,128)(2,1)} %kw_hbm.1, ...), custom_call_target="tpu_custom_call" | custom-call | tf_op jit(solution)/shard_map/pallas_call | solution.py:513
  80.8 3.5 %shard_map.139 = (bf16[1,1280,256]{2,1,0:T(8,128)(2,1)}, bf16[1,1280,256]{2,1,0:T(8,128)(2,1)}, f32[1,2,1280]{2,1,0:T(2,128)}, f32[4,256]{1,0:T(4,128)}) custom-call(bf16[64,2,16,256]{3,2,1,0:T(8,128)(2,1)} %get-tuple-element.8.kv_ref, bf16[256,512]{1,0:T(8,128)(2,1)} %get-tuple-element.9.kvb_ref, f32[2,1280]{1,0:T(2,128)} %get-tuple-element.10.g_ref, ...), custom_call_target="tpu_custom_call" | custom-call | tf_op jit(solution)/shard_map/pallas_call | solution.py:599

commit v4 on v3

--- a/solution.py
+++ b/solution.py
@@ -16,7 +16,24 @@
 MESH = pl.DeviceIdType.MESH
 VMEM = pltpu.VMEM
 
-PAST_AT = (8, 4, 0, 0, 12, 12, 27)
+PAST_AT = (0, 4, 0, 4, 12, 12, 17)
+
+
+def offsets():
+    quarter = [(a, b) for a in range(5) for b in range(5) if a or b]
+    found = []
+    for a, b in sorted(quarter, key=lambda p: -p[0] - p[1]):
+        for p in ((a, b), (-a, -b), (a, -b), (-a, b)):
+            p = (p[0] % NZ, p[1] % NY)
+            if p not in found:
+                found.append(p)
+    return found
+
+
+FAR_FIRST = tuple(offsets())
+ON_RINGS = tuple(p for p in FAR_FIRST if 0 in p)
+OFF_RINGS = tuple(p for p in FAR_FIRST if 0 not in p)
+
 OFFS = (0, -1, 1, -2, 2, -3, 3, -4)
 
 
@@ -70,9 +87,9 @@
     own_v_hbm,
     sg_ref,
     kv_ref,
-    kvb_ref,
-    cg_ref,
-    out_ref,
+    kvb_hbm,
+    cg_hbm,
+    out_hbm,
     src_ref,
     in_ref,
     pg_ref,
@@ -91,6 +108,10 @@
     got_ref,
     part_ref,
     parts_ref,
+    kvb_ref,
+    cg_ref,
+    out_ref,
+    put_sem,
     load_sem,
     kv_send,
     kv_recv,
@@ -122,10 +143,8 @@
         pb = lax.rem(pb + 16, 8)
         return pa * 8 + pb if h == 0 else pb * 8 + pa
 
-    def peer(d):
-        d = lax.rem(d * 45, NSP)
-        dz, dy = d // NY, lax.rem(d, NY)
-        return lax.rem(z + dz, NZ) * NY + lax.rem(y + dy, NY)
+    def peer(offset):
+        return at(0, z + offset[0], y + offset[1])
 
     tp_next = lax.rem(x + 1, NX) * 2 + c
     tp_prev = lax.rem(x + NX - 1, NX) * 2 + c
@@ -302,6 +321,15 @@
                 for side in (1, -1):
                     second_axis(h, off, 0, side)
 
+    def send_past(offset):
+        dest = peer(offset)
+        remote(src_ref.at[dest], kv_ref.at[sp], kv_send, kv_recv, dest, tp).start()
+
+    def stage(n):
+        first = sum(PAST_AT[:n])
+        for offset in OFF_RINGS[first : first + PAST_AT[n]]:
+            send_past(offset)
+
     pass_word()
     pass_word()
     weights_in(1)
@@ -309,31 +337,24 @@
     for d in range(1, 8):
         other = at(0, z, y + d)
         pl.semaphore_signal(rows_in, inc=1, device_id=(other, tp), device_id_type=MESH)
+    for offset in ON_RINGS:
+        send_past(offset)
     weights_in(2)
     pl.semaphore_wait(rows_in, 7)
 
     sends_z = exchange(0, lambda d: lax.rem(z + d, NZ) * NY + y)
 
-    def send_block(d, carry):
-        dest = peer(d)
+    for offset in FAR_FIRST:
+        dest = peer(offset)
         remote(x_ref.at[dest], xg_ref.at[tp, sp], x_send, x_recv, dest, tp).start()
         remote(g_ref.at[dest], go_ref.at[sp], g_send, g_recv, dest, tp).start()
-        return carry
-
-    lax.fori_loop(1, NSP, send_block, 0)
-
-    def send_past(d, b):
-        dest = peer(d)
-        remote(src_ref.at[dest], kv_ref.at[sp], kv_send, kv_recv, dest, tp).start()
-        return b
-
-    def stage(n):
-        first = 1 + sum(PAST_AT[:n])
-        if PAST_AT[n]:
-            lax.fori_loop(first, first + PAST_AT[n], send_past, 0)
 
     xg_ref[tp, sp] = x_ref[sp]
     go_ref[sp] = g_ref[sp]
+    puts = [
+        pltpu.make_async_copy(a, b, put_sem.at[n])
+        for n, (a, b) in enumerate(((kvb_ref, kvb_hbm), (cg_ref, cg_hbm), (out_ref, out_hbm)))
+    ]
     kept = pltpu.make_async_copy(src_ref.at[sp], kv_ref.at[sp], keep_sem)
     kept.start()
     stage(0)
@@ -464,25 +485,25 @@
         jnp.where(lane1 < 32, top[0:1], top[1:2]),
         jnp.where(lane1 < 96, den[0:1], den[1:2]),
     )
-    part_ref[0] = jnp.concatenate([summed[0:1, :128], summed[1:2, 128:], ml, ml], axis=0)
-
-    def send_part(d, carry):
-        remote(part_ref.at[0], parts_ref.at[sp], b_send, b_recv, peer(d), tp).start()
-        return carry
-
-    lax.fori_loop(1, NSP, send_part, 0)
+    for n, piece in enumerate((summed[0:1, :128], summed[1:2, 128:], ml)):
+        part_ref[0, :, n * 128 : (n + 1) * 128] = piece
+
+    for offset in FAR_FIRST:
+        remote(part_ref.at[0], parts_ref.at[sp], b_send, b_recv, peer(offset), tp).start()
     parts_ref[sp] = part_ref[0]
     stage(6)
+    puts[0].start()
+    puts[1].start()
     wait_bytes(parts_ref.at[pl.ds(0, NSP - 1)], b_recv)
     for s in range(4):
         group = pl.ds(s * GROUP, GROUP)
-        marks = parts_ref[group, 2, :]
+        marks = parts_ref[group, 0, 256:384]
         for h in (0, 1):
             m = marks[:, 32 * h : 32 * h + 1]
             top = jnp.max(m, axis=0, keepdims=True)
             f = jnp.exp(m - top)
             den = jnp.sum(marks[:, 64 + 32 * h : 65 + 32 * h] * f, axis=0, keepdims=True)
-            summed = jnp.sum(parts_ref[group, h, :] * f, axis=0, keepdims=True)
+            summed = jnp.sum(parts_ref[group, 0, h * 128 : (h + 1) * 128] * f, axis=0, keepdims=True)
             state[h] = join_row(state[h], s, top, den, summed)
 
     own_k = own_k_ref[...].astype(jnp.float32)
@@ -493,6 +514,7 @@
         score = jnp.broadcast_to(score, (4, 128))
         _, den, summed = merge(state[h], (score, jnp.ones((4, 128), jnp.float32), own_v[:, cols]))
         out_ref[:, cols] = summed / den
+    puts[2].start()
 
     for s in slabs + more + last + sends_z + sends_y:
         s.wait_send()
@@ -503,11 +525,12 @@
     wait_bytes(src_ref.at[pl.ds(0, NSP - 1)], kv_send)
     wait_bytes(src_ref.at[pl.ds(0, NSP - 1)], kv_recv)
     kept.wait()
+    for put in puts:
+        put.wait()
     wait_bytes(parts_ref.at[pl.ds(0, NSP - 1)], b_send)
 
 
 def step(*args):
-    vm = pl.BlockSpec(memory_space=VMEM)
     dma = pltpu.SemaphoreType.DMA
     bf16, f32 = jnp.bfloat16, jnp.float32
     return pl.pallas_call(
@@ -519,7 +542,7 @@
             jax.ShapeDtypeStruct((4, 256), f32),
         ),
         in_specs=[pl.BlockSpec(memory_space=pl.ANY)] * 10 + [pl.BlockSpec(memory_space=pltpu.SMEM)],
-        out_specs=(pl.BlockSpec(memory_space=pl.ANY), vm, vm, vm),
+        out_specs=(pl.BlockSpec(memory_space=pl.ANY),) * 4,
         scratch_shapes=[
             VMEM((NSP, 2, 16, 256), bf16),
             VMEM((256, 512), bf16),
@@ -537,8 +560,12 @@
             VMEM((256, 512), f32),
             VMEM((2, 3, 4, 128), f32),
             VMEM((2, 8, 3, 4, 128), f32),
-            VMEM((1, 4, 128), f32),
-            VMEM((NSP, 4, 128), f32),
+            VMEM((1, 1, 384), f32),
+            VMEM((NSP, 1, 384), f32),
+            VMEM((256, 512), bf16),
+            VMEM((2, NSP * 20), f32),
+            VMEM((4, 256), f32),
+            dma((3,)),
             dma((10,)),
             dma,
             dma,
@@ -593,7 +620,7 @@
 
 
 def settled(kv, kvb, g, o):
-    steps = 4
+    steps = 2
     bf16, f32 = jnp.bfloat16, jnp.float32
     rows = NSP * 20 // steps
     return pl.pallas_call(

time: 84.5 us -> 80.5 us (0.953)
  the two profiles are of different devices: /device:TPU:1 before, /device:TPU:6 now
where the time goes in v4:
time: 80.5 us; the launch traced here: 80.3 us
  Pallas kernels  79.7 us (99%)
    pallas_call x1, Pallas kernels, step(): pl.pallas_call(step_kernel, out_shape=(jax.ShapeDtypeStruct((NSP, 2, 16,...  77.4 us
    pallas_call x1, Pallas kernels, settled(): pl.pallas_call(settle_kernel, grid=(steps,), out_shape=(jax.ShapeDtypeStr...  2.25 us

profile of v4, /device:TPU:6, one launch (start us, length us, event | category | flops | bytes accessed | tf_op | source)
XLA Modules:
  0.0 80.3 jit_solution(7435415668702054413)
XLA Ops:
  0.6 77.4 %shard_map.138 = (bf16[64,2,16,256]{3,2,1,0:T(8,128)(2,1)}, bf16[256,512]{1,0:T(8,128)(2,1)}, f32[2,1280]{1,0:T(2,128)}, f32[4,256]{1,0:T(4,128)}) custom-call(bf16[64,16,256]{2,1,0:T(8,128)(2,1)} %bitcast.4, bf16[64,16,256]{2,1,0:T(8,128)(2,1)} %bitcast.5, bf16[256,512]{1,0:T(8,128)(2,1)} %bitcast.6, bf16[64,256]{1,0:T(8,128)(2,1)} %kw_hbm.1, ...), custom_call_target="tpu_custom_call" | custom-call | tf_op jit(solution)/shard_map/pallas_call | solution.py:536
  78.1 2.2 %shard_map.139 = (bf16[1,1280,256]{2,1,0:T(8,128)(2,1)}, bf16[1,1280,256]{2,1,0:T(8,128)(2,1)}, f32[1,2,1280]{2,1,0:T(2,128)}, f32[4,256]{1,0:T(4,128)}) custom-call(bf16[64,2,16,256]{3,2,1,0:T(8,128)(2,1)} %get-tuple-element.8.kv_ref, bf16[256,512]{1,0:T(8,128)(2,1)} %get-tuple-element.9.kvb_ref, f32[2,1280]{1,0:T(2,128)} %get-tuple-element.10.g_ref, ...), custom_call_target="tpu_custom_call" | custom-call | tf_op jit(solution)/shard_map/pallas_call | solution.py:626

commit v5 on v4

--- a/solution.py
+++ b/solution.py
@@ -337,9 +337,9 @@
     for d in range(1, 8):
         other = at(0, z, y + d)
         pl.semaphore_signal(rows_in, inc=1, device_id=(other, tp), device_id_type=MESH)
+    weights_in(2)
     for offset in ON_RINGS:
         send_past(offset)
-    weights_in(2)
     pl.semaphore_wait(rows_in, 7)
 
     sends_z = exchange(0, lambda d: lax.rem(z + d, NZ) * NY + y)
@@ -347,7 +347,9 @@
     for offset in FAR_FIRST:
         dest = peer(offset)
         remote(x_ref.at[dest], xg_ref.at[tp, sp], x_send, x_recv, dest, tp).start()
-        remote(g_ref.at[dest], go_ref.at[sp], g_send, g_recv, dest, tp).start()
+
+    for offset in FAR_FIRST:
+        remote(g_ref.at[peer(offset)], go_ref.at[sp], g_send, g_recv, peer(offset), tp).start()
 
     xg_ref[tp, sp] = x_ref[sp]
     go_ref[sp] = g_ref[sp]

time: 80.5 us -> 87.1 us (1.082)
  Pallas kernels: 79.7 us -> 86.3 us
    pallas_call x1, Pallas kernels: 77.4 us -> 84.1 us  [step(): pl.pallas_call(step_kernel, out_shape=(jax.ShapeDtypeStruct((NSP, 2, 16,...]
where the time goes in v5:
time: 87.1 us; the launch traced here: 86.9 us
  Pallas kernels  86.3 us (99%)
    pallas_call x1, Pallas kernels, step(): pl.pallas_call(step_kernel, out_shape=(jax.ShapeDtypeStruct((NSP, 2, 16,...  84.1 us
    pallas_call x1, Pallas kernels, settled(): pl.pallas_call(settle_kernel, grid=(steps,), out_shape=(jax.ShapeDtypeStr...  2.25 us

profile of v5, /device:TPU:6, one launch (start us, length us, event | category | flops | bytes accessed | tf_op | source)
XLA Modules:
  0.0 86.9 jit_solution(9207573859315563937)
XLA Ops:
  0.6 84.1 %shard_map.138 = (bf16[64,2,16,256]{3,2,1,0:T(8,128)(2,1)}, bf16[256,512]{1,0:T(8,128)(2,1)}, f32[2,1280]{1,0:T(2,128)}, f32[4,256]{1,0:T(4,128)}) custom-call(bf16[64,16,256]{2,1,0:T(8,128)(2,1)} %bitcast.4, bf16[64,16,256]{2,1,0:T(8,128)(2,1)} %bitcast.5, bf16[256,512]{1,0:T(8,128)(2,1)} %bitcast.6, bf16[64,256]{1,0:T(8,128)(2,1)} %kw_hbm.1, ...), custom_call_target="tpu_custom_call" | custom-call | tf_op jit(solution)/shard_map/pallas_call | solution.py:538
  84.7 2.2 %shard_map.139 = (bf16[1,1280,256]{2,1,0:T(8,128)(2,1)}, bf16[1,1280,256]{2,1,0:T(8,128)(2,1)}, f32[1,2,1280]{2,1,0:T(2,128)}, f32[4,256]{1,0:T(4,128)}) custom-call(bf16[64,2,16,256]{3,2,1,0:T(8,128)(2,1)} %get-tuple-element.8.kv_ref, bf16[256,512]{1,0:T(8,128)(2,1)} %get-tuple-element.9.kvb_ref, f32[2,1280]{1,0:T(2,128)} %get-tuple-element.10.g_ref, ...), custom_call_target="tpu_custom_call" | custom-call | tf_op jit(solution)/shard_map/pallas_call | solution.py:628
